TPU v7x, 256 devices: a whole 4x4x8 slice. The times are simulated.
256 devices in a mesh: sp: 64 (over z, x, core), tp: 4 (over y).
Axes of the slice: x: 4, y: 4, z: 8, core: 2. Of those that a mesh axis runs over, the one named last changes fastest.
Arguments:
- queries: bfloat16 [32768, 2048], P('sp', 'tp'), may hold values from -90 to 90, as said below
- key_rows: bfloat16 [32768, 512], P('sp', 'tp'), may hold values from -6 to 6
- value_rows: bfloat16 [32768, 512], P('sp', 'tp'), may hold values from -6 to 6
- sink_logits: float32 [16], P('tp'), may hold values from 2 to 7
- residual: bfloat16 [32768, 2048], P('sp'), may hold values from -6 to 6
- norm_gain: float32 [2048], replicated, may hold values from 0.1 to 1.9
- out_weight: bfloat16 [2048, 2048], P('tp'), may hold values from -1.5 to 1.5
- gate_weight: bfloat16 [2048, 5632], P('sp', 'tp'), may hold values from -0.125 to 0.125
- up_weight: bfloat16 [2048, 5632], P('sp', 'tp'), may hold values from -0.125 to 0.125
- down_weight: bfloat16 [5632, 2048], P('tp', 'sp'), may hold values from -0.078125 to 0.078125
Outputs:
- mixed: bfloat16 [32768, 2048], P(('sp', 'tp'))
Inputs may be any that keep to these rules, and one draw needn't show every extreme that they name: queries are mostly of order one; some rows may be much larger.
All inputs are finite; a program needn't handle non-finite values.
Results may differ from a plain program's by a relative error of at most 0.012.
Values may be sent and summed in bfloat16 or wider, within the bound.
No kernel may reach another device: no remote copies, remote signals or barrier semaphores. Data moves between devices by JAX's collectives and lax.ppermute only.
A program may use at most 128 MiB of HBM per device.

v0:
```python
import jax
import jax.numpy as jnp
from jax import lax
from jax.sharding import PartitionSpec as P

DH = 128
WIN = 128


EPSILON = 1e-06
MASKED = -1e30


def with_halo(cells, sides, width):
    for axis, dim in sides:
        count = lax.axis_size(axis)
        ends = count - 1
        head = lax.slice_in_dim(cells, 0, width, axis=dim)
        tail = lax.slice_in_dim(cells, cells.shape[dim] - width, cells.shape[dim], axis=dim)
        cells = jnp.concatenate(
            [
                lax.ppermute(tail, axis, [(i, (i + 1) % count) for i in range(ends)]),
                cells,
                lax.ppermute(head, axis, [((i + 1) % count, i) for i in range(ends)]),
            ],
            axis=dim,
        )
    return cells


def split_up(value, dim, size):
    before, after = (value.shape[:dim], value.shape[dim + 1 :])
    return jnp.moveaxis(value.reshape(*before, size, -1, *after), dim, 0)


def sent_and_summed(value, axis, dim):
    size = lax.axis_size(axis)
    blocks = lax.all_to_all(split_up(value, dim, size), axis, 0, 0, tiled=True)
    return jnp.sum(blocks.astype(jnp.float32), axis=0)


def sent_to_all(value, axis):
    size = lax.axis_size(axis)
    return lax.all_to_all(
        jnp.broadcast_to(value[None], (size, *value.shape)), axis, 0, 0, tiled=True
    )


def laid_out(blocks, dim):
    blocks = jnp.moveaxis(blocks, 0, dim)
    lengths = blocks.shape
    return blocks.reshape(*lengths[:dim], lengths[dim] * lengths[dim + 1], *lengths[dim + 2 :])


def gather_directly(value, axis, dim):
    blocks = sent_to_all(value, axis)
    return laid_out(blocks, dim)


def side_by_side(arrays, axis, dim, along):
    ends, at = ([], 0)
    for a in arrays[:-1]:
        at += a.shape[along]
        ends.append(at)
    both = jnp.concatenate(arrays, axis=along)
    return tuple(jnp.split(lax.all_gather(both, axis, axis=dim, tiled=True), ends, axis=along))


def attend_block(query_blk, key_blk, value_blk, sink_logits, query_pos, key_pos, seq_len):
    kv_heads = key_blk.shape[1] // DH
    group_size = query_blk.shape[1] // key_blk.shape[1]
    query_four = query_blk.reshape(query_blk.shape[0], kv_heads, group_size, DH)
    key_three = key_blk.reshape(key_blk.shape[0], kv_heads, DH)
    value_three = value_blk.reshape(value_blk.shape[0], kv_heads, DH)
    scores = jnp.einsum(
        "qhgd,khd->hgqk", query_four, key_three, preferred_element_type=jnp.float32
    ) * DH ** (-0.5)
    allowed = (
        (jnp.abs(key_pos[None, :] - query_pos[:, None]) <= WIN)
        & (key_pos[None, :] >= 0)
        & (key_pos[None, :] < seq_len)
    )
    scores = jnp.where(allowed[None, None], scores, MASKED)
    sink_col = sink_logits.reshape(kv_heads, group_size)[:, :, None]
    highest = jnp.maximum(jnp.max(scores, axis=-1), sink_col)
    weights_exp = jnp.exp(scores - highest[..., None])
    denominator = jnp.sum(weights_exp, axis=-1) + jnp.exp(sink_col - highest)
    probabilities = (weights_exp / denominator[..., None]).astype(jnp.bfloat16)
    heads_out = jnp.einsum(
        "hgqk,khd->qhgd", probabilities, value_three, preferred_element_type=jnp.float32
    )
    return heads_out.astype(jnp.bfloat16).reshape(query_blk.shape[0], kv_heads * group_size * DH)


def rms_scale(rows_wide, norm_gain):
    mean_square = jnp.mean(rows_wide * rows_wide, axis=-1, keepdims=True)
    return (rows_wide * lax.rsqrt(mean_square + EPSILON) * norm_gain).astype(jnp.bfloat16)


def fetch_down(down_weight):
    return lax.all_gather(down_weight, "sp", axis=1, tiled=True)


def shards(
    queries,
    key_rows,
    value_rows,
    sink_logits,
    residual,
    norm_gain,
    out_weight,
    gate_weight,
    up_weight,
    down_weight,
):
    tok_local = queries.shape[0]
    block_len = 2 * WIN
    share_rows = tok_local // lax.axis_size("tp")
    seq_len = tok_local * lax.axis_size("sp")
    device_offset = lax.axis_index("sp") * tok_local
    kv_pair = jnp.stack([key_rows, value_rows])
    kv_ext = with_halo(kv_pair, (("sp", 1),), WIN)

    def one_block(block_index):
        block_first = block_index * block_len
        query_blk = lax.dynamic_slice_in_dim(queries, block_first, block_len, 0)
        key_blk = lax.dynamic_slice_in_dim(kv_ext[0], block_first, block_len + 2 * WIN, 0)
        value_blk = lax.dynamic_slice_in_dim(kv_ext[1], block_first, block_len + 2 * WIN, 0)
        query_pos = device_offset + block_first + jnp.arange(block_len, dtype=jnp.int32)
        key_pos = (
            device_offset + block_first - WIN + jnp.arange(block_len + 2 * WIN, dtype=jnp.int32)
        )
        return attend_block(query_blk, key_blk, value_blk, sink_logits, query_pos, key_pos, seq_len)

    blocks = lax.map(one_block, jnp.arange(tok_local // block_len, dtype=jnp.int32))
    attended = blocks.reshape(tok_local, queries.shape[1])
    own_first = lax.axis_index("tp") * share_rows
    picked = attended
    attn_share = sent_and_summed(
        jnp.dot(picked, out_weight, preferred_element_type=jnp.float32).astype(jnp.bfloat16),
        "tp",
        0,
    )
    middle_own = (
        lax.dynamic_slice_in_dim(residual, own_first, share_rows, 0).astype(jnp.float32)
        + attn_share
    )
    normed_all = gather_directly(rms_scale(middle_own, norm_gain), "tp", 0)
    pieces = side_by_side((gate_weight, up_weight), "sp", 0, 1)
    gate_sectioned = pieces[0]
    up_sectioned = pieces[1]
    gate_acc = jnp.dot(normed_all, gate_sectioned, preferred_element_type=jnp.float32)
    up_acc = jnp.dot(normed_all, up_sectioned, preferred_element_type=jnp.float32)
    down_whole = fetch_down(down_weight)
    hidden = (jax.nn.silu(gate_acc) * up_acc).astype(jnp.bfloat16)
    picked = hidden
    ffn_share = lax.psum_scatter(
        jnp.dot(picked, down_whole, preferred_element_type=jnp.float32).astype(jnp.bfloat16),
        "tp",
        scatter_dimension=0,
        tiled=True,
    ).astype(jnp.float32)
    return (middle_own + ffn_share).astype(jnp.bfloat16)


def solution(mesh):
    placed = (
        P("sp", "tp"),
        P("sp", "tp"),
        P("sp", "tp"),
        P("tp"),
        P("sp", None),
        P(),
        P("tp", None),
        P("sp", "tp"),
        P("sp", "tp"),
        P("tp", "sp"),
    )
    return jax.shard_map(
        shards, mesh=mesh, in_specs=placed, out_specs=P(("sp", "tp"), None), check_vma=False
    )
```

profile of v0, /device:TPU:1, one launch (start us, length us, event | category | flops | bytes accessed | tf_op | source)
XLA Modules:
  0.0 233.1 jit_solution(577112236005821725)
XLA Ops:
  6.5 1.8 pad_maximum_fusion.1
  8.3 0.0 all-gather.5.cloned.1.call-start
  8.4 0.7 all-gather.5.cloned.1.call-update
  9.1 0.8 pad_maximum_fusion.3
  9.9 4.5 %collective-permute-start = (bf16[2,128,128]{2,1,0:T(8,128)(2,1)S(1)}, bf16[2,128,128]{2,1,0:T(8,128)(2,1)S(1)}, u32[]{:S(2)}, u32[]{:S(2)}) collective-permute-start(bf16[2,128,128]{2,1,0:T(8,128)(2,1)S(1)} %get-tuple-element.122), channel_id=1, source_target_pairs={{0,4},{4,8},{8,12},{12,16},{16,20},{20,24},{24,28},{28,32},{32,36}... | collective-permute-start | bytes 196616 | tf_op jit(solution)/shard_map/ppermute | solution.py:22
  14.4 1.9 collective-permute-start.1
  16.4 3.6 %collective-permute-done.1 = bf16[2,128,128]{2,1,0:T(8,128)(2,1)S(1)} collective-permute-done((bf16[2,128,128]{2,1,0:T(8,128)(2,1)S(1)}, bf16[2,128,128]{2,1,0:T(8,128)(2,1)S(1)}, u32[]{:S(2)}, u32[]{:S(2)}) %collective-permute-start.1) | collective-permute-done | bytes 65568 | tf_op jit(solution)/shard_map/ppermute | solution.py:24
  20.0 1.0 pad_maximum_fusion
  21.0 11.1 %while.12 = (s32[]{:T(128)}, bf16[2,256,512]{2,1,0:T(8,128)(2,1)}, bf16[2,768,128]{2,1,0:T(8,128)(2,1)S(1)}, s32[2]{0:T(128)S(1)}, s32[]{:T(128)}, /*index=5*/bf...) while((s32[]{:T(128)}, bf16[2,256,512]{2,1,0:T(8,128)(2,1)}, ...), condition=%wide.region_3.4_spmd, body=%wide.region_0.3_spmd.sunk | while | flops 273420544 | bytes 14467520 | solution.py:135
  21.0 0.6 dynamic_slice.48
  22.3 0.3 fusion.46
  22.6 1.0 constant_dynamic-slice_fusion.2
  23.6 0.1 copy.25
  23.7 0.5 fusion.47
  24.2 0.1 broadcast_maximum_fusion.2
  24.3 0.3 fusion.48
  24.6 0.1 exponential_add_fusion.2
  24.7 0.5 convolution_convert_fusion.4
  25.2 0.1 copy.26
  25.4 0.4 copy-done.4
  25.8 0.8 copy-done.5
  26.6 0.6 dynamic_slice.48
  27.8 0.3 fusion.46
  28.1 1.0 constant_dynamic-slice_fusion.2
  29.1 0.1 copy.25
  29.3 0.5 fusion.47
  29.8 0.1 broadcast_maximum_fusion.2
  29.8 0.3 fusion.48
  30.1 0.1 exponential_add_fusion.2
  30.2 0.5 convolution_convert_fusion.4
  30.8 0.1 copy.26
  30.9 0.4 copy-done.4
  31.3 0.8 copy-done.5
  32.1 3.6 %convolution_convert_fusion.1 = bf16[512,2048]{1,0:T(8,128)(2,1)} fusion(bf16[512,512]{1,0:T(8,128)(2,1)} %bitcast.59, bf16[512,2048]{1,0:T(8,128)(2,1)S(1)} %copy-done), kind=kOutput, calls=%fused_computation.30 | convolution fusion | flops 1074790400 | bytes 4718592 | tf_op jit(solution)/shard_map/dot_general | solution.py:140
  35.7 4.4 %all-to-all-start = ((bf16[4,128,2048]{2,1,0:T(8,128)(2,1)}), bf16[4,128,2048]{2,1,0:T(8,128)(2,1)}, u32[]{:S(2)}, u32[]{:S(2)}) async-start(bf16[4,128,2048]{2,1,0:T(8,128)(2,1)} %bitcast.52), calls=%async_computation | async-start | bytes 4194304 | tf_op jit(solution)/shard_map/all_to_all | solution.py:38
  40.2 0.0 reduce-scatter.2.cloned.1.call-start
  40.2 24.7 %all-to-all-done = bf16[4,128,2048]{2,1,0:T(8,128)(2,1)} async-done(((bf16[4,128,2048]{2,1,0:T(8,128)(2,1)}), bf16[4,128,2048]{2,1,0:T(8,128)(2,1)}, u32[]{:S(2)}, u32[]{:S(2)}) %all-to-all-start) | async-done | bytes 2097184 | tf_op jit(solution)/shard_map/all_to_all | solution.py:38
  64.9 2.2 convert_reduce_fusion
  67.2 0.2 multiply_reduce_fusion
  67.4 0.2 multiply_convert_fusion
  67.6 0.2 broadcast_in_dim.44
  67.9 30.0 %all_to_all.10 = bf16[4,128,2048]{2,1,0:T(8,128)(2,1)} all-to-all(bf16[4,128,2048]{2,1,0:T(8,128)(2,1)S(1)} %broadcast_in_dim.44), channel_id=1, replica_groups=mesh['sp'=64,'tp'=4] {'tp'}, dimensions={0} | all-to-all | bytes 4194304 | tf_op jit(solution)/shard_map/all_to_all | solution.py:44
  97.9 4.1 %all-gather.3.cloned.1.call-done = bf16[2048,2816]{1,0:T(8,128)(2,1)} async-done(((bf16[32,2816]{1,0:T(8,128)(2,1)}), bf16[2048,2816]{1,0:T(8,128)(2,1)}) %all-gather.3.cloned.1.call-update) | async-done | bytes 11534352 | tf_op jit(solution)/shard_map/all_gather | solution.py:66
  102.0 8.2 %fusion.14 = f32[512,1408]{1,0:T(8,128)} fusion(bf16[512,2048]{1,0:T(8,128)(2,1)} %bitcast.53, bf16[2048,2816]{1,0:T(8,128)(2,1)} %all-gather.3.cloned.1.call-done), kind=kOutput, calls=%fused_computation.25 | convolution fusion | flops 2952790016 | bytes 10747904 | tf_op jit(solution)/shard_map/dot_general | solution.py:152
  110.2 71.3 %all-gather.5.cloned.1.call-done = bf16[1408,2048]{0,1:T(8,128)(2,1)} async-done(((bf16[1408,32]{0,1:T(8,128)(2,1)}), bf16[1408,2048]{0,1:T(8,128)(2,1)}) %all-gather.5.cloned.1.call-update) | async-done | bytes 5767184 | tf_op jit(solution)/shard_map/all_gather | solution.py:101
  181.5 13.8 %convolution_convert_fusion.2 = bf16[512,2048]{1,0:T(8,128)(2,1)} fusion(bf16[1408,2048]{0,1:T(8,128)(2,1)} %all-gather.5.cloned.1.call-done, bf16[512,2048]{1,0:T(8,128)(2,1)} %bitcast.54, bf16[2048,2816]{1,0:T(8,128)(2,1)} %all-gather.3.cloned.1.call-done, f32[512,1408]{1,0:T(8,128)} %fusion.14), kind=kOutput, calls=%fused_computation.31 | convolution fusion | flops 5910953984 | bytes 18612224 | tf_op jit(solution)/shard_map/dot_general | solution.py:158
  195.4 29.0 %reduce-scatter.2.cloned.1.call-done = bf16[128,2048]{1,0:T(8,128)(2,1)} async-done(((bf16[512,2048]{1,0:T(8,128)(2,1)}), bf16[128,2048]{1,0:T(8,128)(2,1)}) %reduce-scatter.2.cloned.1.call-update) | async-done | bytes 524304 | tf_op jit(solution)/shard_map/reduce_scatter | solution.py:157
  224.4 2.2 add_convert_fusion
  (31 shorter events, 0.2 us)
Async XLA Ops:
  6.5 25.6 %copy-start = (bf16[512,2048]{1,0:T(8,128)(2,1)S(1)}, bf16[512,2048]{1,0:T(8,128)(2,1)}, u32[]{:S(2)}) copy-start(bf16[512,2048]{1,0:T(8,128)(2,1)} %param.18) | copy-start | bytes 6291460
  6.5 95.5 %all-gather.3.cloned.1.call-start = ((), (), s32[]{:S(2)}) async-start(), calls=%async_computation.3 | async-start | bytes 11714560 | tf_op jit(solution)/shard_map/all_gather | solution.py:66
  8.3 173.2 %all-gather.5.cloned.1.call-start = ((), (), s32[]{:S(2)}) async-start(), calls=%async_computation.4 | async-start | bytes 5857280 | tf_op jit(solution)/shard_map/all_gather | solution.py:101
  9.9 6.5 %collective-permute-start = (bf16[2,128,128]{2,1,0:T(8,128)(2,1)S(1)}, bf16[2,128,128]{2,1,0:T(8,128)(2,1)S(1)}, u32[]{:S(2)}, u32[]{:S(2)}) collective-permute-start(bf16[2,128,128]{2,1,0:T(8,128)(2,1)S(1)} %get-tuple-element.122), channel_id=1, source_target_pairs={{0,4},{4,8},{8,12},{12,16},{16,20},{20,24},{24,28},{28,32},{32,36}... | collective-permute-start | bytes 196616 | tf_op jit(solution)/shard_map/ppermute | solution.py:22
  14.4 5.6 %collective-permute-start.1 = (bf16[2,128,128]{2,1,0:T(8,128)(2,1)S(1)}, bf16[2,128,128]{2,1,0:T(8,128)(2,1)S(1)}, u32[]{:S(2)}, u32[]{:S(2)}) collective-permute-start(bf16[2,128,128]{2,1,0:T(8,128)(2,1)S(1)} %get-tuple-element.123), channel_id=1, source_target_pairs={{4,0},{8,4},{12,8},{16,12},{20,16},{24,20},{28,24},{32,28},{36,32}... | collective-permute-start | bytes 196616 | tf_op jit(solution)/shard_map/ppermute | solution.py:24
  23.6 0.7 copy-start.2
  24.7 1.0 copy-start.4
  25.8 0.8 copy-start.5
  29.1 0.7 copy-start.2
  30.2 1.0 copy-start.4
  31.3 0.8 copy-start.5
  35.7 29.2 %all-to-all-start = ((bf16[4,128,2048]{2,1,0:T(8,128)(2,1)}), bf16[4,128,2048]{2,1,0:T(8,128)(2,1)}, u32[]{:S(2)}, u32[]{:S(2)}) async-start(bf16[4,128,2048]{2,1,0:T(8,128)(2,1)} %bitcast.52), calls=%async_computation | async-start | bytes 4194304 | tf_op jit(solution)/shard_map/all_to_all | solution.py:38
  40.2 184.2 %reduce-scatter.2.cloned.1.call-start = ((), (), s32[]{:S(2)}) async-start(), calls=%async_computation.5 | async-start | bytes 2621440 | tf_op jit(solution)/shard_map/reduce_scatter | solution.py:157
  40.2 27.2 %copy-start.3 = (f32[2048]{0:T(1024)S(1)}, f32[2048]{0:T(1024)}, u32[]{:S(2)}) copy-start(f32[2048]{0:T(1024)} %param.17) | copy-start | bytes 24580
  64.9 2.2 copy-start.1
Sparse Core Ops, SparseCore 0:
  10.1 91.8 all-gather.2
  104.7 76.7 all-gather.4
  195.5 28.8 reduce-scatter.1
where the time goes:
time: 234 us; the launch traced here: 233 us
  waiting for transfers between devices  133 us (57%)
  blocking collectives  30 us (13%)
  matrix products  27.7 us (12%)
  between operations  13.2 us (6%)
  starting transfers between devices  10.9 us (5%)
  other arithmetic  9.91 us (4%)
  local copies, waits for them, and re-layouts  6.4 us (3%)
    all_gather x1, waiting for transfers between devices, fetch_down(): return lax.all_gather(down_weight, 'sp', axis=1, tiled=True)  71.3 us
    all_to_all x1, blocking collectives, sent_to_all(): lax.all_to_all(jnp.broadcast_to(value[None], (size, *value.shape)), axis,...  30 us
    reduce_scatter x1, waiting for transfers between devices, shards(): lax.psum_scatter(jnp.dot(picked, down_whole, preferred_element_type=jnp.f...  29 us
    all_to_all x1, waiting for transfers between devices, sent_and_summed(): blocks = lax.all_to_all(split_up(value, dim, size), axis, 0, 0, tiled=True)  24.7 us
    dot_general x1, matrix products, shards(): jnp.dot(picked, down_whole, preferred_element_type=jnp.float32)  13.8 us
    dot_general x1, matrix products, shards(): jnp.dot(normed_all, gate_sectioned, preferred_element_type=jnp.float32)  8.23 us
  transfers between devices with their start and end apart: 6, of which 5 were waited for; matrix products, arithmetic and copies ran while one was open for 10% of the time, Pallas kernels for 0%

commit v1 on v0

--- a/solution.py
+++ b/solution.py
@@ -97,8 +97,39 @@
     return (rows_wide * lax.rsqrt(mean_square + EPSILON) * norm_gain).astype(jnp.bfloat16)
 
 
-def fetch_down(down_weight):
-    return lax.all_gather(down_weight, "sp", axis=1, tiled=True)
+def hop(value, step):
+    size = lax.axis_size("tp")
+    return lax.ppermute(value, "tp", [(i, (i + step) % size) for i in range(size)])
+
+
+def ring_sum(parts):
+    half = parts.shape[1] // 2
+    me = lax.axis_index("tp")
+    own = lax.dynamic_index_in_dim(parts, me, 0, keepdims=False)
+    nxt = lax.dynamic_index_in_dim(parts, (me + 1) % 4, 0, keepdims=False)
+    prv = lax.dynamic_index_in_dim(parts, (me + 3) % 4, 0, keepdims=False)
+    far = lax.dynamic_index_in_dim(parts, (me + 2) % 4, 0, keepdims=False)
+    up = hop(far[:half], 1)
+    down = hop(far[half:], -1)
+    up_sum = (nxt[:half].astype(jnp.float32) + up.astype(jnp.float32)).astype(jnp.bfloat16)
+    down_sum = (prv[half:].astype(jnp.float32) + down.astype(jnp.float32)).astype(jnp.bfloat16)
+    from_prev = hop(jnp.concatenate([up_sum, nxt[half:]]), 1)
+    from_next = hop(jnp.concatenate([prv[:half], down_sum]), -1)
+    return (
+        own.astype(jnp.float32) + from_prev.astype(jnp.float32) + from_next.astype(jnp.float32)
+    )
+
+
+def ring_gather(own):
+    half = own.shape[0] // 2
+    left = hop(own, 1)
+    right = hop(own, -1)
+    far_a = hop(left[:half], 1)
+    far_b = hop(right[half:], -1)
+    far = jnp.concatenate([far_a, far_b])
+    me = lax.axis_index("tp")
+    rel = jnp.stack([own, right, far, left])
+    return jnp.concatenate([lax.dynamic_index_in_dim(rel, (k - me) % 4, 0, keepdims=False) for k in range(4)])
 
 
 def shards(
@@ -136,30 +167,31 @@
     attended = blocks.reshape(tok_local, queries.shape[1])
     own_first = lax.axis_index("tp") * share_rows
     picked = attended
-    attn_share = sent_and_summed(
-        jnp.dot(picked, out_weight, preferred_element_type=jnp.float32).astype(jnp.bfloat16),
-        "tp",
-        0,
+    attn_share = ring_sum(
+        jnp.dot(picked, out_weight, preferred_element_type=jnp.float32)
+        .astype(jnp.bfloat16)
+        .reshape(4, share_rows, -1)
     )
     middle_own = (
         lax.dynamic_slice_in_dim(residual, own_first, share_rows, 0).astype(jnp.float32)
         + attn_share
     )
-    normed_all = gather_directly(rms_scale(middle_own, norm_gain), "tp", 0)
-    pieces = side_by_side((gate_weight, up_weight), "sp", 0, 1)
+    normed_all = ring_gather(rms_scale(middle_own, norm_gain))
+    pieces = side_by_side((gate_weight, up_weight, down_weight.T), "sp", 0, 1)
     gate_sectioned = pieces[0]
     up_sectioned = pieces[1]
     gate_acc = jnp.dot(normed_all, gate_sectioned, preferred_element_type=jnp.float32)
     up_acc = jnp.dot(normed_all, up_sectioned, preferred_element_type=jnp.float32)
-    down_whole = fetch_down(down_weight)
+    down_whole = pieces[2]
     hidden = (jax.nn.silu(gate_acc) * up_acc).astype(jnp.bfloat16)
     picked = hidden
-    ffn_share = lax.psum_scatter(
-        jnp.dot(picked, down_whole, preferred_element_type=jnp.float32).astype(jnp.bfloat16),
-        "tp",
-        scatter_dimension=0,
-        tiled=True,
-    ).astype(jnp.float32)
+    ffn_share = ring_sum(
+        lax.dot_general(
+            picked, down_whole, (((1,), (1,)), ((), ())), preferred_element_type=jnp.float32
+        )
+        .astype(jnp.bfloat16)
+        .reshape(4, share_rows, -1)
+    )
     return (middle_own + ffn_share).astype(jnp.bfloat16)
 
 

time: 234 us -> 172 us (0.74)
  waiting for transfers between devices: 133 us -> 85.8 us
  blocking collectives: 30 us -> 0 us
  starting transfers between devices: 10.9 us -> 20.6 us
  local copies, waits for them, and re-layouts: 6.4 us -> 11 us
    all_gather x1 -> x0, waiting for transfers between devices: 71.3 us -> none  [fetch_down(): return lax.all_gather(down_weight, 'sp', axis=1, tiled=True)]
    ppermute x0 -> x12, waiting for transfers between devices: none -> 58.6 us  [hop(): lax.ppermute(value, 'tp', [(i, (i + step) % size) for i in range(size)])]
    all_to_all x1 -> x0, blocking collectives: 30 us -> none  [sent_to_all(): lax.all_to_all(jnp.broadcast_to(value[None], (size, *value.shape)), axis,...]
    reduce_scatter x1 -> x0, waiting for transfers between devices: 29 us -> none  [shards(): lax.psum_scatter(jnp.dot(picked, down_whole, preferred_element_type=jnp.f...]
    all_to_all x1 -> x0, waiting for transfers between devices: 24.7 us -> none  [sent_and_summed(): blocks = lax.all_to_all(split_up(value, dim, size), axis, 0, 0, tiled=True)]
    all_gather x1, waiting for transfers between devices: 4.12 us -> 23.6 us  [side_by_side(): lax.all_gather(both, axis, axis=dim, tiled=True)]
    ppermute x0 -> x12, starting transfers between devices: none -> 14.1 us  [hop(): lax.ppermute(value, 'tp', [(i, (i + step) % size) for i in range(size)])]
    all_to_all x1 -> x0, starting transfers between devices: 4.43 us -> none  [sent_and_summed(): blocks = lax.all_to_all(split_up(value, dim, size), axis, 0, 0, tiled=True)]
  transfers between devices with their start and end apart: 6 -> 15, of which waited for: 5 -> 12; matrix products, arithmetic and copies ran while one was open for 10% -> 13% of each run, Pallas kernels for 0% -> 0%
where the time goes in v1:
time: 172 us; the launch traced here: 171 us
  waiting for transfers between devices  85.8 us (50%)
  matrix products  26.5 us (15%)
  starting transfers between devices  20.6 us (12%)
  between operations  13.7 us (8%)
  other arithmetic  12.1 us (7%)
  local copies, waits for them, and re-layouts  11 us (6%)
    ppermute x12, waiting for transfers between devices, hop(): lax.ppermute(value, 'tp', [(i, (i + step) % size) for i in range(size)])  58.6 us
    all_gather x1, waiting for transfers between devices, side_by_side(): lax.all_gather(both, axis, axis=dim, tiled=True)  23.6 us
    ppermute x12, starting transfers between devices, hop(): lax.ppermute(value, 'tp', [(i, (i + step) % size) for i in range(size)])  14.1 us
    dot_general x1, matrix products, shards(): lax.dot_general(picked, down_whole, (((1,), (1,)), ((), ())), preferred_e...  13.9 us
    dot_general x1, matrix products, shards(): jnp.dot(normed_all, gate_sectioned, preferred_element_type=jnp.float32)  8.26 us
    ppermute x1, starting transfers between devices, with_halo(): lax.ppermute(tail, axis, [(i, (i + 1) % count) for i in range(ends)])  4.5 us
    ppermute x1, waiting for transfers between devices, with_halo(): lax.ppermute(head, axis, [((i + 1) % count, i) for i in range(ends)])  3.57 us
  transfers between devices with their start and end apart: 15, of which 12 were waited for; matrix products, arithmetic and copies ran while one was open for 13% of the time, Pallas kernels for 0%

profile of v1, /device:TPU:1, one launch (start us, length us, event | category | flops | bytes accessed | tf_op | source)
XLA Modules:
  0.0 171.1 jit_solution(12854896761295459989)
XLA Ops:
  6.5 1.9 %pad_maximum_fusion.10 = bf16[32,4224]{1,0:T(8,128)(2,1)} fusion(bf16[32,1408]{1,0:T(8,128)(2,1)} %bitcast.117, bf16[32,1408]{1,0:T(8,128)(2,1)} %param.20, bf16[32,1408]{1,0:T(8,128)(2,1)} %param.19), kind=kLoop, calls=%fused_computation.63 | loop fusion | flops 811008 | bytes 540672 | tf_op jit(solution)/shard_map/concatenate | solution.py:65
  8.4 0.8 pad_maximum_fusion.12
  9.2 4.5 %collective-permute-start = (bf16[2,128,128]{2,1,0:T(8,128)(2,1)S(1)}, bf16[2,128,128]{2,1,0:T(8,128)(2,1)S(1)}, u32[]{:S(2)}, u32[]{:S(2)}) collective-permute-start(bf16[2,128,128]{2,1,0:T(8,128)(2,1)S(1)} %get-tuple-element.140), channel_id=1, source_target_pairs={{0,4},{4,8},{8,12},{12,16},{16,20},{20,24},{24,28},{28,32},{32,36}... | collective-permute-start | bytes 196616 | tf_op jit(solution)/shard_map/ppermute | solution.py:22
  13.7 1.9 %collective-permute-start.1 = (bf16[2,128,128]{2,1,0:T(8,128)(2,1)S(1)}, bf16[2,128,128]{2,1,0:T(8,128)(2,1)S(1)}, u32[]{:S(2)}, u32[]{:S(2)}) collective-permute-start(bf16[2,128,128]{2,1,0:T(8,128)(2,1)S(1)} %get-tuple-element.141), channel_id=1, source_target_pairs={{4,0},{8,4},{12,8},{16,12},{20,16},{24,20},{28,24},{32,28},{36,32}... | collective-permute-start | bytes 196616 | tf_op jit(solution)/shard_map/ppermute | solution.py:24
  15.8 3.6 %collective-permute-done.1 = bf16[2,128,128]{2,1,0:T(8,128)(2,1)S(1)} collective-permute-done((bf16[2,128,128]{2,1,0:T(8,128)(2,1)S(1)}, bf16[2,128,128]{2,1,0:T(8,128)(2,1)S(1)}, u32[]{:S(2)}, u32[]{:S(2)}) %collective-permute-start.1) | collective-permute-done | bytes 65568 | tf_op jit(solution)/shard_map/ppermute | solution.py:24
  19.3 1.0 pad_maximum_fusion.6
  20.4 10.3 %while.12 = (s32[]{:T(128)}, bf16[2,256,512]{2,1,0:T(8,128)(2,1)}, bf16[2,768,128]{2,1,0:T(8,128)(2,1)S(1)}, s32[2]{0:T(128)S(1)}, s32[]{:T(128)}, /*index=5*/bf...) while((s32[]{:T(128)}, bf16[2,256,512]{2,1,0:T(8,128)(2,1)}, ...), condition=%wide.region_3.4_spmd, body=%wide.region_0.3_spmd.sunk | while | flops 273420544 | bytes 10273068 | solution.py:166
  20.4 0.7 dynamic_slice.99
  22.0 1.0 constant_dynamic-slice_fusion.2
  23.1 0.5 fusion.64
  24.1 0.5 convolution_convert_fusion.3
  24.8 0.7 constant_dynamic-update-slice_fusion.2
  25.5 0.6 dynamic_slice.99
  27.1 1.0 constant_dynamic-slice_fusion.2
  28.3 0.5 fusion.64
  29.2 0.5 convolution_convert_fusion.3
  29.9 0.7 constant_dynamic-update-slice_fusion.2
  30.7 2.3 %convolution_convert_fusion.1 = bf16[512,2048]{1,0:T(8,128)(2,1)S(1)} fusion(bf16[512,512]{1,0:T(8,128)(2,1)} %bitcast.118, bf16[512,2048]{1,0:T(8,128)(2,1)S(1)} %copy-done), kind=kOutput, calls=%fused_computation.31 | convolution fusion | flops 1074790400 | bytes 4718592 | tf_op jit(solution)/shard_map/dot_general | solution.py:171
  33.1 1.4 collective-permute-start.2
  34.4 1.5 collective-permute-start.4
  36.0 4.8 %collective-permute-done.2 = bf16[64,2048]{1,0:T(8,128)(2,1)S(1)} collective-permute-done((bf16[64,2048]{1,0:T(8,128)(2,1)S(1)}, bf16[64,2048]{1,0:T(8,128)(2,1)S(1)}, u32[]{:S(2)}, u32[]{:S(2)}) %collective-permute-start.2) | collective-permute-done | bytes 262176 | tf_op jit(solution)/shard_map/ppermute | solution.py:102
  41.3 2.6 %collective-permute-start.5 = (bf16[128,2048]{1,0:T(8,128)(2,1)S(1)}, bf16[128,2048]{1,0:T(8,128)(2,1)S(1)}, u32[]{:S(2)}, u32[]{:S(2)}) collective-permute-start(bf16[128,2048]{1,0:T(8,128)(2,1)S(1)} %pad_maximum_fusion.3), channel_id=1, source_target_pairs={{0,3},{1,0},{2,1},{3,2},{4,7},{5,4},{6,5},{7,6},{8,11},{9,8},{10,9... | collective-permute-start | bytes 1572872 | tf_op jit(solution)/shard_map/ppermute | solution.py:102
  44.0 0.8 pad_maximum_fusion.2
  44.8 9.8 %collective-permute-done.5 = bf16[128,2048]{1,0:T(8,128)(2,1)S(1)} collective-permute-done((bf16[128,2048]{1,0:T(8,128)(2,1)S(1)}, bf16[128,2048]{1,0:T(8,128)(2,1)S(1)}, u32[]{:S(2)}, u32[]{:S(2)}) %collective-permute-start.5) | collective-permute-done | bytes 524320 | tf_op jit(solution)/shard_map/ppermute | solution.py:102
  54.6 0.8 copy-done.3
  55.4 3.8 %collective-permute-done.3 = bf16[128,2048]{1,0:T(8,128)(2,1)} collective-permute-done((bf16[128,2048]{1,0:T(8,128)(2,1)}, bf16[128,2048]{1,0:T(8,128)(2,1)}, u32[]{:S(2)}, u32[]{:S(2)}) %collective-permute-start.3) | collective-permute-done | bytes 524320 | tf_op jit(solution)/shard_map/ppermute | solution.py:102
  59.2 2.0 %multiply_reduce_fusion = (f32[128]{0:T(128)S(1)}, f32[128,2048]{1,0:T(8,128)S(1)}) fusion(bf16[128,2048]{1,0:T(8,128)(2,1)} %copy-done.3, bf16[128,2048]{1,0:T(8,128)(2,1)} %collective-permute-done.3, bf16[4,128,2048]{2,1,0:T(8,128)(2,1)} %bitcast.109, s32[]{:T(128)S(6)} %select_n.90, bf16[512,2048]{1,0:T(8,128)(2,1)} %param.16, s32[]{:T(128)S(6)} %select_n.89), kind=kLoop, calls=%fused_computation.44 | loop fusion | flops 2359168 | bytes 3146248 | tf_op jit(solution)/shard_map/reduce_sum | solution.py:96
  61.2 0.9 multiply_convert_fusion
  62.1 1.5 collective-permute-start.7
  63.6 12.4 %collective-permute-done.6 = bf16[128,2048]{1,0:T(8,128)(2,1)} collective-permute-done((bf16[128,2048]{1,0:T(8,128)(2,1)}, bf16[128,2048]{1,0:T(8,128)(2,1)}, u32[]{:S(2)}, u32[]{:S(2)}) %collective-permute-start.6) | collective-permute-done | bytes 524320 | tf_op jit(solution)/shard_map/ppermute | solution.py:102
  76.1 1.0 slice.113
  77.0 1.6 collective-permute-start.9
  78.6 1.0 slice.112
  80.0 4.3 %collective-permute-done.9 = bf16[64,2048]{1,0:T(8,128)(2,1)S(1)} collective-permute-done((bf16[64,2048]{1,0:T(8,128)(2,1)S(1)}, bf16[64,2048]{1,0:T(8,128)(2,1)S(1)}, u32[]{:S(2)}, u32[]{:S(2)}) %collective-permute-start.9) | collective-permute-done | bytes 262176 | tf_op jit(solution)/shard_map/ppermute | solution.py:102
  84.3 3.9 %collective-permute-done.8 = bf16[64,2048]{1,0:T(8,128)(2,1)S(1)} collective-permute-done((bf16[64,2048]{1,0:T(8,128)(2,1)S(1)}, bf16[64,2048]{1,0:T(8,128)(2,1)S(1)}, u32[]{:S(2)}, u32[]{:S(2)}) %collective-permute-start.8) | collective-permute-done | bytes 262176 | tf_op jit(solution)/shard_map/ppermute | solution.py:102
  88.3 1.5 pad_maximum_fusion
  89.8 1.4 dynamic-slice_bitcast_fusion.3
  91.2 23.6 %all-gather.2.cloned.1.call-done = bf16[2048,4224]{1,0:T(8,128)(2,1)} async-done(((bf16[32,4224]{1,0:T(8,128)(2,1)}), bf16[2048,4224]{1,0:T(8,128)(2,1)}) %all-gather.2.cloned.1.call-update) | async-done | bytes 17301520 | tf_op jit(solution)/shard_map/all_gather | solution.py:66
  114.8 8.3 %fusion.16 = f32[512,1408]{1,0:T(8,128)} fusion(bf16[2048,4224]{1,0:T(8,128)(2,1)} %all-gather.2.cloned.1.call-done, bf16[128,2048]{1,0:T(8,128)(2,1)} %get-tuple-element.131, bf16[128,2048]{1,0:T(8,128)(2,1)} %get-tuple-element.132, bf16[128,2048]{1,0:T(8,128)(2,1)} %get-tuple-element.133, bf16[128,2048]{1,0:T(8,128)(2,1)} %get-tuple-element.130), kind=kOutput, calls=%fused_computation.27 | convolution fusion | flops 2961178624 | bytes 10747904 | tf_op jit(solution)/shard_map/dot_general | solution.py:183
  123.1 13.9 %fusion.24 = bf16[512,2048]{1,0:T(8,128)(2,1)} fusion(bf16[2048,4224]{1,0:T(8,128)(2,1)} %all-gather.2.cloned.1.call-done, f32[512,1408]{1,0:T(8,128)} %fusion.16, bf16[128,2048]{1,0:T(8,128)(2,1)} %get-tuple-element.131, bf16[128,2048]{1,0:T(8,128)(2,1)} %get-tuple-element.132, bf16[128,2048]{1,0:T(8,128)(2,1)} %get-tuple-element.133, ...), kind=kOutput, calls=%fused_computation.32 | convolution fusion | flops 5919342592 | bytes 18612224 | tf_op jit(solution)/shard_map/dot_general | solution.py:189
  137.0 1.4 dynamic-slice_bitcast_fusion.8
  138.4 1.3 collective-permute-start.10
  139.7 1.5 collective-permute-start.12
  141.2 6.1 %collective-permute-done.10 = bf16[64,2048]{1,0:T(8,128)(2,1)S(1)} collective-permute-done((bf16[64,2048]{1,0:T(8,128)(2,1)S(1)}, bf16[64,2048]{1,0:T(8,128)(2,1)S(1)}, u32[]{:S(2)}, u32[]{:S(2)}) %collective-permute-start.10) | collective-permute-done | bytes 262176 | tf_op jit(solution)/shard_map/ppermute | solution.py:102
  147.5 2.5 %collective-permute-start.13 = (bf16[128,2048]{1,0:T(8,128)(2,1)S(1)}, bf16[128,2048]{1,0:T(8,128)(2,1)S(1)}, u32[]{:S(2)}, u32[]{:S(2)}) collective-permute-start(bf16[128,2048]{1,0:T(8,128)(2,1)S(1)} %pad_maximum_fusion.5), channel_id=1, source_target_pairs={{0,3},{1,0},{2,1},{3,2},{4,7},{5,4},{6,5},{7,6},{8,11},{9,8},{10,9... | collective-permute-start | bytes 1572872 | tf_op jit(solution)/shard_map/ppermute | solution.py:102
  150.1 9.8 %collective-permute-done.13 = bf16[128,2048]{1,0:T(8,128)(2,1)S(1)} collective-permute-done((bf16[128,2048]{1,0:T(8,128)(2,1)S(1)}, bf16[128,2048]{1,0:T(8,128)(2,1)S(1)}, u32[]{:S(2)}, u32[]{:S(2)}) %collective-permute-start.13) | collective-permute-done | bytes 524320 | tf_op jit(solution)/shard_map/ppermute | solution.py:102
  159.9 3.2 %collective-permute-done.11 = bf16[128,2048]{1,0:T(8,128)(2,1)S(1)} collective-permute-done((bf16[128,2048]{1,0:T(8,128)(2,1)S(1)}, bf16[128,2048]{1,0:T(8,128)(2,1)S(1)}, u32[]{:S(2)}, u32[]{:S(2)}) %collective-permute-start.11) | collective-permute-done | bytes 524320 | tf_op jit(solution)/shard_map/ppermute | solution.py:102
  163.1 1.1 fusion.32
  (52 shorter events, 3.5 us)
Async XLA Ops:
  6.5 24.1 %copy-start = (bf16[512,2048]{1,0:T(8,128)(2,1)S(1)}, bf16[512,2048]{1,0:T(8,128)(2,1)}, u32[]{:S(2)}) copy-start(bf16[512,2048]{1,0:T(8,128)(2,1)} %param.18) | copy-start | bytes 6291460
  6.5 13.8 %copy-start.4 = (f32[4]{0:T(128)S(1)}, f32[4]{0:T(128)}, u32[]{:S(2)}) copy-start(f32[4]{0:T(128)} %param.15) | copy-start | bytes 52
  6.5 108.3 %all-gather.2.cloned.1.call-start = ((), (), s32[]{:S(2)}) async-start(), calls=%async_computation | async-start | bytes 17571840 | tf_op jit(solution)/shard_map/all_gather | solution.py:66
  9.2 6.5 %collective-permute-start = (bf16[2,128,128]{2,1,0:T(8,128)(2,1)S(1)}, bf16[2,128,128]{2,1,0:T(8,128)(2,1)S(1)}, u32[]{:S(2)}, u32[]{:S(2)}) collective-permute-start(bf16[2,128,128]{2,1,0:T(8,128)(2,1)S(1)} %get-tuple-element.140), channel_id=1, source_target_pairs={{0,4},{4,8},{8,12},{12,16},{16,20},{20,24},{24,28},{28,32},{32,36}... | collective-permute-start | bytes 196616 | tf_op jit(solution)/shard_map/ppermute | solution.py:22
  13.7 5.6 %collective-permute-start.1 = (bf16[2,128,128]{2,1,0:T(8,128)(2,1)S(1)}, bf16[2,128,128]{2,1,0:T(8,128)(2,1)S(1)}, u32[]{:S(2)}, u32[]{:S(2)}) collective-permute-start(bf16[2,128,128]{2,1,0:T(8,128)(2,1)S(1)} %get-tuple-element.141), channel_id=1, source_target_pairs={{4,0},{8,4},{12,8},{16,12},{20,16},{24,20},{28,24},{32,28},{36,32}... | collective-permute-start | bytes 196616 | tf_op jit(solution)/shard_map/ppermute | solution.py:24
  33.0 8.4 %copy-start.1 = (bf16[512,2048]{1,0:T(8,128)(2,1)}, bf16[512,2048]{1,0:T(8,128)(2,1)S(1)}, u32[]{:S(2)}) copy-start(bf16[512,2048]{1,0:T(8,128)(2,1)S(1)} %convolution_convert_fusion.1) | copy-start | bytes 6291460
  33.1 7.7 %collective-permute-start.2 = (bf16[64,2048]{1,0:T(8,128)(2,1)S(1)}, bf16[64,2048]{1,0:T(8,128)(2,1)S(1)}, u32[]{:S(2)}, u32[]{:S(2)}) collective-permute-start(bf16[64,2048]{1,0:T(8,128)(2,1)S(1)} %get-tuple-element.136), channel_id=1, source_target_pairs={{0,1},{1,2},{2,3},{3,0},{4,5},{5,6},{6,7},{7,4},{8,9},{9,10},{10,1... | collective-permute-start | bytes 786440 | tf_op jit(solution)/shard_map/ppermute | solution.py:102
  34.4 6.7 %collective-permute-start.4 = (bf16[64,2048]{1,0:T(8,128)(2,1)S(1)}, bf16[64,2048]{1,0:T(8,128)(2,1)S(1)}, u32[]{:S(2)}, u32[]{:S(2)}) collective-permute-start(bf16[64,2048]{1,0:T(8,128)(2,1)S(1)} %get-tuple-element.138), channel_id=1, source_target_pairs={{0,3},{1,0},{2,1},{3,2},{4,7},{5,4},{6,5},{7,6},{8,11},{9,8},{10,9... | collective-permute-start | bytes 786440 | tf_op jit(solution)/shard_map/ppermute | solution.py:102
  41.3 13.3 %collective-permute-start.5 = (bf16[128,2048]{1,0:T(8,128)(2,1)S(1)}, bf16[128,2048]{1,0:T(8,128)(2,1)S(1)}, u32[]{:S(2)}, u32[]{:S(2)}) collective-permute-start(bf16[128,2048]{1,0:T(8,128)(2,1)S(1)} %pad_maximum_fusion.3), channel_id=1, source_target_pairs={{0,3},{1,0},{2,1},{3,2},{4,7},{5,4},{6,5},{7,6},{8,11},{9,8},{10,9... | collective-permute-start | bytes 1572872 | tf_op jit(solution)/shard_map/ppermute | solution.py:102
  44.0 17.2 %copy-start.5 = (f32[2048]{0:T(1024)S(1)}, f32[2048]{0:T(1024)}, u32[]{:S(2)}) copy-start(f32[2048]{0:T(1024)} %param.17) | copy-start | bytes 24580
  44.8 14.4 %collective-permute-start.3 = (bf16[128,2048]{1,0:T(8,128)(2,1)}, bf16[128,2048]{1,0:T(8,128)(2,1)}, u32[]{:S(2)}, u32[]{:S(2)}) collective-permute-start(bf16[128,2048]{1,0:T(8,128)(2,1)} %pad_maximum_fusion.2), channel_id=1, source_target_pairs={{0,1},{1,2},{2,3},{3,0},{4,5},{5,6},{6,7},{7,4},{8,9},{9,10},{10,1... | collective-permute-start | bytes 1572872 | tf_op jit(solution)/shard_map/ppermute | solution.py:102
  54.6 0.8 copy-start.3
  62.1 13.9 %collective-permute-start.6 = (bf16[128,2048]{1,0:T(8,128)(2,1)}, bf16[128,2048]{1,0:T(8,128)(2,1)}, u32[]{:S(2)}, u32[]{:S(2)}) collective-permute-start(bf16[128,2048]{1,0:T(8,128)(2,1)} %multiply_convert_fusion), channel_id=1, source_target_pairs={{0,3},{1,0},{2,1},{3,2},{4,7},{5,4},{6,5},{7,6},{8,11},{9,8},{10,9... | collective-permute-start | bytes 1572872 | tf_op jit(solution)/shard_map/ppermute | solution.py:102
  62.1 16.4 %collective-permute-start.7 = (bf16[128,2048]{1,0:T(8,128)(2,1)}, bf16[128,2048]{1,0:T(8,128)(2,1)}, u32[]{:S(2)}, u32[]{:S(2)}) collective-permute-start(bf16[128,2048]{1,0:T(8,128)(2,1)} %multiply_convert_fusion), channel_id=1, source_target_pairs={{0,1},{1,2},{2,3},{3,0},{4,5},{5,6},{6,7},{7,4},{8,9},{9,10},{10,1... | collective-permute-start | bytes 1572872 | tf_op jit(solution)/shard_map/ppermute | solution.py:102
  77.0 7.3 %collective-permute-start.9 = (bf16[64,2048]{1,0:T(8,128)(2,1)S(1)}, bf16[64,2048]{1,0:T(8,128)(2,1)S(1)}, u32[]{:S(2)}, u32[]{:S(2)}) collective-permute-start(bf16[64,2048]{1,0:T(8,128)(2,1)S(1)} %slice.113), channel_id=1, source_target_pairs={{0,3},{1,0},{2,1},{3,2},{4,7},{5,4},{6,5},{7,6},{8,11},{9,8},{10,9... | collective-permute-start | bytes 786440 | tf_op jit(solution)/shard_map/ppermute | solution.py:102
  79.6 8.7 %collective-permute-start.8 = (bf16[64,2048]{1,0:T(8,128)(2,1)S(1)}, bf16[64,2048]{1,0:T(8,128)(2,1)S(1)}, u32[]{:S(2)}, u32[]{:S(2)}) collective-permute-start(bf16[64,2048]{1,0:T(8,128)(2,1)S(1)} %slice.112), channel_id=1, source_target_pairs={{0,1},{1,2},{2,3},{3,0},{4,5},{5,6},{6,7},{7,4},{8,9},{9,10},{10,1... | collective-permute-start | bytes 786440 | tf_op jit(solution)/shard_map/ppermute | solution.py:102
  137.0 10.3 %copy-start.2 = (bf16[512,2048]{1,0:T(8,128)(2,1)S(1)}, bf16[512,2048]{1,0:T(8,128)(2,1)}, u32[]{:S(2)}) copy-start(bf16[512,2048]{1,0:T(8,128)(2,1)} %fusion.24) | copy-start | bytes 6291460
  138.4 8.9 %collective-permute-start.10 = (bf16[64,2048]{1,0:T(8,128)(2,1)S(1)}, bf16[64,2048]{1,0:T(8,128)(2,1)S(1)}, u32[]{:S(2)}, u32[]{:S(2)}) collective-permute-start(bf16[64,2048]{1,0:T(8,128)(2,1)S(1)} %get-tuple-element.126), channel_id=1, source_target_pairs={{0,1},{1,2},{2,3},{3,0},{4,5},{5,6},{6,7},{7,4},{8,9},{9,10},{10,1... | collective-permute-start | bytes 786440 | tf_op jit(solution)/shard_map/ppermute | solution.py:102
  139.7 7.6 %collective-permute-start.12 = (bf16[64,2048]{1,0:T(8,128)(2,1)S(1)}, bf16[64,2048]{1,0:T(8,128)(2,1)S(1)}, u32[]{:S(2)}, u32[]{:S(2)}) collective-permute-start(bf16[64,2048]{1,0:T(8,128)(2,1)S(1)} %get-tuple-element.128), channel_id=1, source_target_pairs={{0,3},{1,0},{2,1},{3,2},{4,7},{5,4},{6,5},{7,6},{8,11},{9,8},{10,9... | collective-permute-start | bytes 786440 | tf_op jit(solution)/shard_map/ppermute | solution.py:102
  147.5 12.4 %collective-permute-start.13 = (bf16[128,2048]{1,0:T(8,128)(2,1)S(1)}, bf16[128,2048]{1,0:T(8,128)(2,1)S(1)}, u32[]{:S(2)}, u32[]{:S(2)}) collective-permute-start(bf16[128,2048]{1,0:T(8,128)(2,1)S(1)} %pad_maximum_fusion.5), channel_id=1, source_target_pairs={{0,3},{1,0},{2,1},{3,2},{4,7},{5,4},{6,5},{7,6},{8,11},{9,8},{10,9... | collective-permute-start | bytes 1572872 | tf_op jit(solution)/shard_map/ppermute | solution.py:102
  150.0 13.1 %collective-permute-start.11 = (bf16[128,2048]{1,0:T(8,128)(2,1)S(1)}, bf16[128,2048]{1,0:T(8,128)(2,1)S(1)}, u32[]{:S(2)}, u32[]{:S(2)}) collective-permute-start(bf16[128,2048]{1,0:T(8,128)(2,1)S(1)} %pad_maximum_fusion.4), channel_id=1, source_target_pairs={{0,1},{1,2},{2,3},{3,0},{4,5},{5,6},{6,7},{7,4},{8,9},{9,10},{10,1... | collective-permute-start | bytes 1572872 | tf_op jit(solution)/shard_map/ppermute | solution.py:102
Sparse Core Ops, SparseCore 0:
  10.1 104.6 all-gather.1

commit v2 on v1

--- a/solution.py
+++ b/solution.py
@@ -1,6 +1,8 @@
 import jax
 import jax.numpy as jnp
 from jax import lax
+from jax.experimental import pallas as pl
+from jax.experimental.pallas import tpu as pltpu
 from jax.sharding import PartitionSpec as P
 
 DH = 128
@@ -28,44 +30,6 @@
     return cells
 
 
-def split_up(value, dim, size):
-    before, after = (value.shape[:dim], value.shape[dim + 1 :])
-    return jnp.moveaxis(value.reshape(*before, size, -1, *after), dim, 0)
-
-
-def sent_and_summed(value, axis, dim):
-    size = lax.axis_size(axis)
-    blocks = lax.all_to_all(split_up(value, dim, size), axis, 0, 0, tiled=True)
-    return jnp.sum(blocks.astype(jnp.float32), axis=0)
-
-
-def sent_to_all(value, axis):
-    size = lax.axis_size(axis)
-    return lax.all_to_all(
-        jnp.broadcast_to(value[None], (size, *value.shape)), axis, 0, 0, tiled=True
-    )
-
-
-def laid_out(blocks, dim):
-    blocks = jnp.moveaxis(blocks, 0, dim)
-    lengths = blocks.shape
-    return blocks.reshape(*lengths[:dim], lengths[dim] * lengths[dim + 1], *lengths[dim + 2 :])
-
-
-def gather_directly(value, axis, dim):
-    blocks = sent_to_all(value, axis)
-    return laid_out(blocks, dim)
-
-
-def side_by_side(arrays, axis, dim, along):
-    ends, at = ([], 0)
-    for a in arrays[:-1]:
-        at += a.shape[along]
-        ends.append(at)
-    both = jnp.concatenate(arrays, axis=along)
-    return tuple(jnp.split(lax.all_gather(both, axis, axis=dim, tiled=True), ends, axis=along))
-
-
 def attend_block(query_blk, key_blk, value_blk, sink_logits, query_pos, key_pos, seq_len):
     kv_heads = key_blk.shape[1] // DH
     group_size = query_blk.shape[1] // key_blk.shape[1]
@@ -120,16 +84,71 @@
     )
 
 
-def ring_gather(own):
-    half = own.shape[0] // 2
-    left = hop(own, 1)
-    right = hop(own, -1)
-    far_a = hop(left[:half], 1)
-    far_b = hop(right[half:], -1)
-    far = jnp.concatenate([far_a, far_b])
-    me = lax.axis_index("tp")
-    rel = jnp.stack([own, right, far, left])
-    return jnp.concatenate([lax.dynamic_index_in_dim(rel, (k - me) % 4, 0, keepdims=False) for k in range(4)])
+FF_LOCAL = 1408
+STEPS = ((0, 256), (256, 256), (512, 256), (768, 256), (1024, 256), (1280, 128))
+
+
+def ffn_kernel(own, nxt, far_lo, far_hi, prv, w, *refs):
+    outs, mine, (hidden, wg, wd, sems) = refs[:6], refs[6], refs[7:]
+
+    def fetch(part, first, width, to, sem):
+        src = w.at[:, pl.ds(part * FF_LOCAL + first, width)]
+        return pltpu.make_async_copy(src, to, sem)
+
+    copies = []
+    for n, (first, width) in enumerate(STEPS):
+        for part in range(2):
+            to = wg.at[:, pl.ds(2 * first + part * width, width)]
+            copies.append(fetch(part, first, width, to, sems.at[2 * n + part]))
+    downs = fetch(2, 0, FF_LOCAL, wd, sems.at[12])
+    for c in copies + [downs]:
+        c.start()
+    x = jnp.concatenate([far_lo[...], far_hi[...], nxt[...], prv[...], own[...]], axis=0)
+    for n, (first, width) in enumerate(STEPS):
+        copies[2 * n].wait()
+        copies[2 * n + 1].wait()
+        acc = jnp.dot(
+            x, wg[:, 2 * first : 2 * (first + width)], preferred_element_type=jnp.float32
+        )
+        gate = acc[:, :width]
+        hid = gate / (1.0 + jnp.exp(-gate)) * acc[:, width:]
+        hidden[:, first : first + width] = hid.astype(jnp.bfloat16)
+    downs.wait()
+    res = lax.dot_general(
+        hidden[...], wd[...], (((1,), (1,)), ((), ())), preferred_element_type=jnp.float32
+    )
+    for i, out in enumerate(outs):
+        out[...] = res[64 * i : 64 * i + 64].astype(jnp.bfloat16)
+    mine[...] = res[384:]
+
+
+def bf16(*shape):
+    return jax.ShapeDtypeStruct(shape, jnp.bfloat16)
+
+
+def feed_forward(own, nxt, far_lo, far_hi, prv, weights):
+    vmem = pl.BlockSpec(memory_space=pltpu.VMEM)
+    hbm = pl.BlockSpec(memory_space=pltpu.HBM)
+    out_lo, out_hi, nxt_lo, nxt_hi, prv_lo, prv_hi, mine = pl.pallas_call(
+        ffn_kernel,
+        out_shape=(bf16(64, 2048),) * 6 + (jax.ShapeDtypeStruct((128, 2048), jnp.float32),),
+        in_specs=[vmem] * 5 + [hbm],
+        out_specs=(vmem,) * 7,
+        scratch_shapes=[
+            pltpu.VMEM((512, FF_LOCAL), jnp.bfloat16),
+            pltpu.VMEM((2048, 2 * FF_LOCAL), jnp.bfloat16),
+            pltpu.VMEM((2048, FF_LOCAL), jnp.bfloat16),
+            pltpu.SemaphoreType.DMA((13,)),
+        ],
+        compiler_params=pltpu.CompilerParams(vmem_limit_bytes=36 * 1024 * 1024),
+        name="ffn",
+    )(own, nxt, far_lo, far_hi, prv, weights)
+    up, down = hop(out_lo, 1), hop(out_hi, -1)
+    prev_hi, next_lo = hop(nxt_hi, 1), hop(prv_lo, -1)
+    up_sum = (nxt_lo.astype(jnp.float32) + up.astype(jnp.float32)).astype(jnp.bfloat16)
+    down_sum = (prv_hi.astype(jnp.float32) + down.astype(jnp.float32)).astype(jnp.bfloat16)
+    prev_lo, next_hi = hop(up_sum, 1), hop(down_sum, -1)
+    return mine, prev_lo, prev_hi, next_lo, next_hi
 
 
 def shards(
@@ -176,21 +195,20 @@
         lax.dynamic_slice_in_dim(residual, own_first, share_rows, 0).astype(jnp.float32)
         + attn_share
     )
-    normed_all = ring_gather(rms_scale(middle_own, norm_gain))
-    pieces = side_by_side((gate_weight, up_weight, down_weight.T), "sp", 0, 1)
-    gate_sectioned = pieces[0]
-    up_sectioned = pieces[1]
-    gate_acc = jnp.dot(normed_all, gate_sectioned, preferred_element_type=jnp.float32)
-    up_acc = jnp.dot(normed_all, up_sectioned, preferred_element_type=jnp.float32)
-    down_whole = pieces[2]
-    hidden = (jax.nn.silu(gate_acc) * up_acc).astype(jnp.bfloat16)
-    picked = hidden
-    ffn_share = ring_sum(
-        lax.dot_general(
-            picked, down_whole, (((1,), (1,)), ((), ())), preferred_element_type=jnp.float32
-        )
-        .astype(jnp.bfloat16)
-        .reshape(4, share_rows, -1)
+    normed = rms_scale(middle_own, norm_gain)
+    prv, nxt = hop(normed, 1), hop(normed, -1)
+    far_lo, far_hi = hop(prv[:64], 1), hop(nxt[64:], -1)
+    weights = lax.all_gather(
+        jnp.concatenate([gate_weight, up_weight, down_weight.T], axis=1), "sp", axis=0, tiled=True
+    )
+    mine, prev_lo, prev_hi, next_lo, next_hi = feed_forward(
+        normed, nxt, far_lo, far_hi, prv, weights
+    )
+    ffn_share = mine + jnp.concatenate(
+        [
+            prev_lo.astype(jnp.float32) + next_lo.astype(jnp.float32),
+            prev_hi.astype(jnp.float32) + next_hi.astype(jnp.float32),
+        ]
     )
     return (middle_own + ffn_share).astype(jnp.bfloat16)
 

time: 172 us -> 162 us (0.942)
  matrix products: 26.5 us -> 4.33 us
  Pallas kernels: 0 us -> 13.8 us
  starting transfers between devices: 20.6 us -> 25.7 us
  waiting for transfers between devices: 85.8 us -> 81 us
  other arithmetic: 12.1 us -> 9.97 us
    dot_general x2 -> x0, matrix products: 22.2 us -> none  [the longest x1 13.9 us: shards(): lax.dot_general(picked, down_whole, (((1,), (1,)), ((), ())), preferred_e...]
    pallas_call x0 -> x1, Pallas kernels: none -> 13.8 us  [feed_forward(): pl.pallas_call(ffn_kernel, out_shape=(bf16(64, 2048),) * 6 + (jax.ShapeDt...]
    ppermute x12 -> x14, waiting for transfers between devices: 58.6 us -> 48.8 us  [hop(): lax.ppermute(value, 'tp', [(i, (i + step) % size) for i in range(size)])]
    ppermute x12 -> x14, starting transfers between devices: 14.1 us -> 19.2 us  [hop(): lax.ppermute(value, 'tp', [(i, (i + step) % size) for i in range(size)])]
    all_gather x1, waiting for transfers between devices: 23.6 us -> 28.6 us  [shards(): lax.all_gather(jnp.concatenate([gate_weight, up_weight, down_weight.T], a...]
    unnamed x12 -> x20, local copies, waits for them, and re-layouts: 0.81 us -> 3.52 us
    while x0 -> x8, local copies, waits for them, and re-layouts: none -> 2.29 us
    slice x2, local copies, waits for them, and re-layouts: 1.94 us -> 0.04 us  [shards(): far_lo, far_hi = (hop(prv[:64], 1), hop(nxt[64:], -1))]
  transfers between devices with their start and end apart: 15 -> 17, of which waited for: 12 -> 12; matrix products, arithmetic and copies ran while one was open for 13% -> 10% of each run, Pallas kernels for 0% -> 0%
where the time goes in v2:
time: 162 us; the launch traced here: 160 us
  waiting for transfers between devices  81 us (50%)
  starting transfers between devices  25.7 us (16%)
  Pallas kernels  13.8 us (9%)
  between operations  13.7 us (8%)
  other arithmetic  9.97 us (6%)
  local copies, waits for them, and re-layouts  9.84 us (6%)
  matrix products  4.33 us (3%)
    ppermute x14, waiting for transfers between devices, hop(): lax.ppermute(value, 'tp', [(i, (i + step) % size) for i in range(size)])  48.8 us
    all_gather x1, waiting for transfers between devices, shards(): lax.all_gather(jnp.concatenate([gate_weight, up_weight, down_weight.T], a...  28.6 us
    ppermute x14, starting transfers between devices, hop(): lax.ppermute(value, 'tp', [(i, (i + step) % size) for i in range(size)])  19.2 us
    pallas_call x1, Pallas kernels, feed_forward(): pl.pallas_call(ffn_kernel, out_shape=(bf16(64, 2048),) * 6 + (jax.ShapeDt...  13.8 us
    ppermute x1, starting transfers between devices, with_halo(): lax.ppermute(tail, axis, [(i, (i + 1) % count) for i in range(ends)])  4.5 us
    ppermute x1, waiting for transfers between devices, with_halo(): lax.ppermute(head, axis, [((i + 1) % count, i) for i in range(ends)])  3.57 us
    unnamed x20, local copies, waits for them, and re-layouts  3.52 us
  transfers between devices with their start and end apart: 17, of which 12 were waited for; matrix products, arithmetic and copies ran while one was open for 10% of the time, Pallas kernels for 0%

profile of v2, /device:TPU:1, one launch (start us, length us, event | category | flops | bytes accessed | tf_op | source)
XLA Modules:
  0.0 159.9 jit_solution(18228678447397552373)
XLA Ops:
  6.5 1.9 %pad_maximum_fusion.3 = bf16[32,4224]{1,0:T(8,128)(2,1)} fusion(bf16[32,1408]{1,0:T(8,128)(2,1)} %bitcast.78, bf16[32,1408]{1,0:T(8,128)(2,1)} %param.20, bf16[32,1408]{1,0:T(8,128)(2,1)} %param.19), kind=kLoop, calls=%fused_computation.43 | loop fusion | flops 811008 | bytes 540672 | tf_op jit(solution)/shard_map/concatenate | solution.py:202
  8.4 0.8 pad_maximum_fusion.5
  9.2 4.5 %collective-permute-start = (bf16[2,128,128]{2,1,0:T(8,128)(2,1)S(1)}, bf16[2,128,128]{2,1,0:T(8,128)(2,1)S(1)}, u32[]{:S(2)}, u32[]{:S(2)}) collective-permute-start(bf16[2,128,128]{2,1,0:T(8,128)(2,1)S(1)} %get-tuple-element.144), channel_id=1, source_target_pairs={{0,4},{4,8},{8,12},{12,16},{16,20},{20,24},{24,28},{28,32},{32,36}... | collective-permute-start | bytes 196616 | tf_op jit(solution)/shard_map/ppermute | solution.py:24
  13.7 1.9 %collective-permute-start.1 = (bf16[2,128,128]{2,1,0:T(8,128)(2,1)S(1)}, bf16[2,128,128]{2,1,0:T(8,128)(2,1)S(1)}, u32[]{:S(2)}, u32[]{:S(2)}) collective-permute-start(bf16[2,128,128]{2,1,0:T(8,128)(2,1)S(1)} %get-tuple-element.145), channel_id=1, source_target_pairs={{4,0},{8,4},{12,8},{16,12},{20,16},{24,20},{28,24},{32,28},{36,32}... | collective-permute-start | bytes 196616 | tf_op jit(solution)/shard_map/ppermute | solution.py:26
  15.8 3.6 %collective-permute-done.1 = bf16[2,128,128]{2,1,0:T(8,128)(2,1)S(1)} collective-permute-done((bf16[2,128,128]{2,1,0:T(8,128)(2,1)S(1)}, bf16[2,128,128]{2,1,0:T(8,128)(2,1)S(1)}, u32[]{:S(2)}, u32[]{:S(2)}) %collective-permute-start.1) | collective-permute-done | bytes 65568 | tf_op jit(solution)/shard_map/ppermute | solution.py:26
  19.3 1.0 pad_maximum_fusion.2
  20.4 11.3 %while.12 = (s32[]{:T(128)}, bf16[2,256,512]{2,1,0:T(8,128)(2,1)}, bf16[2,768,128]{2,1,0:T(8,128)(2,1)S(1)}, s32[2]{0:T(128)S(1)}, s32[]{:T(128)}, /*index=5*/bf...) while((s32[]{:T(128)}, bf16[2,256,512]{2,1,0:T(8,128)(2,1)}, ...), condition=%wide.region_3.4_spmd, body=%wide.region_0.3_spmd.sunk | while | flops 273420544 | bytes 14467428 | solution.py:185
  20.4 0.7 dynamic_slice.62
  22.1 1.0 constant_dynamic-slice_fusion.2
  23.2 0.5 fusion.38
  24.1 0.5 convolution_convert_fusion.3
  25.2 0.8 copy-done.11
  26.0 0.7 dynamic_slice.62
  27.7 1.0 constant_dynamic-slice_fusion.2
  28.9 0.5 fusion.38
  29.8 0.5 convolution_convert_fusion.3
  30.5 0.4 copy-done.10
  30.9 0.8 copy-done.11
  31.7 2.3 %convolution_convert_fusion.1 = bf16[512,2048]{1,0:T(8,128)(2,1)S(1)} fusion(bf16[512,512]{1,0:T(8,128)(2,1)} %bitcast.79, bf16[512,2048]{1,0:T(8,128)(2,1)S(1)} %copy-done), kind=kOutput, calls=%fused_computation.23 | convolution fusion | flops 1074790400 | bytes 4718592 | tf_op jit(solution)/shard_map/dot_general | solution.py:190
  34.1 1.4 collective-permute-start.2
  35.4 1.5 collective-permute-start.4
  37.0 4.4 %collective-permute-done.2 = bf16[64,2048]{1,0:T(8,128)(2,1)S(1)} collective-permute-done((bf16[64,2048]{1,0:T(8,128)(2,1)S(1)}, bf16[64,2048]{1,0:T(8,128)(2,1)S(1)}, u32[]{:S(2)}, u32[]{:S(2)}) %collective-permute-start.2) | collective-permute-done | bytes 262176 | tf_op jit(solution)/shard_map/ppermute | solution.py:66
  41.4 0.4 collective-permute-done.4
  42.0 0.8 pad_maximum_fusion.1
  42.8 2.6 %collective-permute-start.5 = (bf16[128,2048]{1,0:T(8,128)(2,1)}, bf16[128,2048]{1,0:T(8,128)(2,1)S(1)}, u32[]{:S(2)}, u32[]{:S(2)}) collective-permute-start(bf16[128,2048]{1,0:T(8,128)(2,1)} %pad_maximum_fusion.1), channel_id=1, source_target_pairs={{0,3},{1,0},{2,1},{3,2},{4,7},{5,4},{6,5},{7,6},{8,11},{9,8},{10,9... | collective-permute-start | bytes 1572872 | tf_op jit(solution)/shard_map/ppermute | solution.py:66
  45.4 0.8 pad_maximum_fusion
  46.2 10.5 %collective-permute-done.5 = bf16[128,2048]{1,0:T(8,128)(2,1)S(1)} collective-permute-done((bf16[128,2048]{1,0:T(8,128)(2,1)}, bf16[128,2048]{1,0:T(8,128)(2,1)S(1)}, u32[]{:S(2)}, u32[]{:S(2)}) %collective-permute-start.5) | collective-permute-done | bytes 524320 | tf_op jit(solution)/shard_map/ppermute | solution.py:66
  56.7 4.1 %collective-permute-done.3 = bf16[128,2048]{1,0:T(8,128)(2,1)S(1)} collective-permute-done((bf16[128,2048]{1,0:T(8,128)(2,1)}, bf16[128,2048]{1,0:T(8,128)(2,1)S(1)}, u32[]{:S(2)}, u32[]{:S(2)}) %collective-permute-start.3) | collective-permute-done | bytes 524320 | tf_op jit(solution)/shard_map/ppermute | solution.py:66
  60.8 1.6 multiply_reduce_fusion
  62.7 2.7 %collective-permute-start.6 = (bf16[128,2048]{1,0:T(8,128)(2,1)S(1)}, bf16[128,2048]{1,0:T(8,128)(2,1)S(1)}, u32[]{:S(2)}, u32[]{:S(2)}) collective-permute-start(bf16[128,2048]{1,0:T(8,128)(2,1)S(1)} %multiply_convert_fusion.own), channel_id=1, source_target_pairs={{0,3},{1,0},{2,1},{3,2},{4,7},{5,4},{6,5},{7,6},{8,11},{9,8},{10,9... | collective-permute-start | bytes 1572872 | tf_op jit(solution)/shard_map/ppermute | solution.py:66
  65.4 11.9 %collective-permute-done.7.prv = bf16[128,2048]{1,0:T(8,128)(2,1)S(1)} collective-permute-done((bf16[128,2048]{1,0:T(8,128)(2,1)S(1)}, bf16[128,2048]{1,0:T(8,128)(2,1)S(1)}, u32[]{:S(2)}, u32[]{:S(2)}) %collective-permute-start.7) | collective-permute-done | bytes 524320 | tf_op jit(solution)/shard_map/ppermute | solution.py:66
  77.4 0.8 copy-done.1
  78.2 2.7 %collective-permute-start.9 = (bf16[64,2048]{1,0:T(8,128)(2,1)S(1)}, bf16[64,2048]{1,0:T(8,128)(2,1)S(1)}, u32[]{:S(2)}, u32[]{:S(2)}) collective-permute-start(bf16[64,2048]{1,0:T(8,128)(2,1)S(1)} %slice.71), channel_id=1, source_target_pairs={{0,3},{1,0},{2,1},{3,2},{4,7},{5,4},{6,5},{7,6},{8,11},{9,8},{10,9... | collective-permute-start | bytes 786440 | tf_op jit(solution)/shard_map/ppermute | solution.py:66
  80.8 4.7 %collective-permute-done.8.far_lo = bf16[64,2048]{1,0:T(8,128)(2,1)S(1)} collective-permute-done((bf16[64,2048]{1,0:T(8,128)(2,1)S(1)}, bf16[64,2048]{1,0:T(8,128)(2,1)S(1)}, u32[]{:S(2)}, u32[]{:S(2)}) %collective-permute-start.8) | collective-permute-done | bytes 262176 | tf_op jit(solution)/shard_map/ppermute | solution.py:66
  85.5 0.7 copy-done.3
  86.2 28.6 %all-gather.2.cloned.1.call-done.w = bf16[2048,4224]{1,0:T(8,128)(2,1)} async-done(((bf16[32,4224]{1,0:T(8,128)(2,1)}), bf16[2048,4224]{1,0:T(8,128)(2,1)}) %all-gather.2.cloned.1.call-update) | async-done | bytes 17301520 | tf_op jit(solution)/shard_map/all_gather | solution.py:201
  114.8 1.0 copy-done.2
  115.9 0.9 copy-done.4
  116.8 13.8 %ffn.1 = (bf16[64,2048]{1,0:T(8,128)(2,1)S(1)}, bf16[64,2048]{1,0:T(8,128)(2,1)S(1)}, bf16[64,2048]{1,0:T(8,128)(2,1)S(1)}, bf16[64,2048]{1,0:T(8,128)(2,1)S(1)}...) custom-call(bf16[128,2048]{1,0:T(8,128)(2,1)S(1)} %multiply_convert_fusion.own, ...), custom_call_target="tpu_custom_call" | custom-call | tf_op jit(solution)/shard_map/ffn/pallas_call | solution.py:132
  130.6 1.3 collective-permute-start.10
  131.9 1.5 collective-permute-start.12
  133.4 2.7 %collective-permute-start.14 = (bf16[64,2048]{1,0:T(8,128)(2,1)S(1)}, bf16[64,2048]{1,0:T(8,128)(2,1)S(1)}, u32[]{:S(2)}, u32[]{:S(2)}) collective-permute-start(bf16[64,2048]{1,0:T(8,128)(2,1)S(1)} %get-tuple-element.108), channel_id=1, source_target_pairs={{0,3},{1,0},{2,1},{3,2},{4,7},{5,4},{6,5},{7,6},{8,11},{9,8},{10,9... | collective-permute-start | bytes 786440 | tf_op jit(solution)/shard_map/ppermute | solution.py:66
  136.0 3.5 %collective-permute-done.10 = bf16[64,2048]{1,0:T(8,128)(2,1)S(1)} collective-permute-done((bf16[64,2048]{1,0:T(8,128)(2,1)S(1)}, bf16[64,2048]{1,0:T(8,128)(2,1)S(1)}, u32[]{:S(2)}, u32[]{:S(2)}) %collective-permute-start.10) | collective-permute-done | bytes 262176 | tf_op jit(solution)/shard_map/ppermute | solution.py:66
  139.7 5.2 %collective-permute-done.14 = bf16[64,2048]{1,0:T(8,128)(2,1)S(1)} collective-permute-done((bf16[64,2048]{1,0:T(8,128)(2,1)S(1)}, bf16[64,2048]{1,0:T(8,128)(2,1)S(1)}, u32[]{:S(2)}, u32[]{:S(2)}) %collective-permute-start.14) | collective-permute-done | bytes 262176 | tf_op jit(solution)/shard_map/ppermute | solution.py:66
  144.9 2.7 %collective-permute-start.15 = (bf16[64,2048]{1,0:T(8,128)(2,1)S(1)}, bf16[64,2048]{1,0:T(8,128)(2,1)S(1)}, u32[]{:S(2)}, u32[]{:S(2)}) collective-permute-start(bf16[64,2048]{1,0:T(8,128)(2,1)S(1)} %add_convert_fusion), channel_id=1, source_target_pairs={{0,3},{1,0},{2,1},{3,2},{4,7},{5,4},{6,5},{7,6},{8,11},{9,8},{10,9... | collective-permute-start | bytes 786440 | tf_op jit(solution)/shard_map/ppermute | solution.py:66
  147.7 3.1 %collective-permute-done.11 = bf16[64,2048]{1,0:T(8,128)(2,1)S(1)} collective-permute-done((bf16[64,2048]{1,0:T(8,128)(2,1)S(1)}, bf16[64,2048]{1,0:T(8,128)(2,1)S(1)}, u32[]{:S(2)}, u32[]{:S(2)}) %collective-permute-start.11) | collective-permute-done | bytes 262176 | tf_op jit(solution)/shard_map/ppermute | solution.py:66
  150.8 1.1 collective-permute-done.15
  152.0 1.0 fusion.13
  (67 shorter events, 3.5 us)
Async XLA Ops:
  6.5 25.1 %copy-start = (bf16[512,2048]{1,0:T(8,128)(2,1)S(1)}, bf16[512,2048]{1,0:T(8,128)(2,1)}, u32[]{:S(2)}) copy-start(bf16[512,2048]{1,0:T(8,128)(2,1)} %param.18) | copy-start | bytes 6291460
  6.5 13.8 %copy-start.8 = (f32[4]{0:T(128)S(1)}, f32[4]{0:T(128)}, u32[]{:S(2)}) copy-start(f32[4]{0:T(128)} %param.15) | copy-start | bytes 52
  6.5 108.3 %all-gather.2.cloned.1.call-start = ((), (), s32[]{:S(2)}) async-start(), calls=%async_computation | async-start | bytes 17571840 | tf_op jit(solution)/shard_map/all_gather | solution.py:201
  9.2 6.5 %collective-permute-start = (bf16[2,128,128]{2,1,0:T(8,128)(2,1)S(1)}, bf16[2,128,128]{2,1,0:T(8,128)(2,1)S(1)}, u32[]{:S(2)}, u32[]{:S(2)}) collective-permute-start(bf16[2,128,128]{2,1,0:T(8,128)(2,1)S(1)} %get-tuple-element.144), channel_id=1, source_target_pairs={{0,4},{4,8},{8,12},{12,16},{16,20},{20,24},{24,28},{28,32},{32,36}... | collective-permute-start | bytes 196616 | tf_op jit(solution)/shard_map/ppermute | solution.py:24
  13.7 5.6 %collective-permute-start.1 = (bf16[2,128,128]{2,1,0:T(8,128)(2,1)S(1)}, bf16[2,128,128]{2,1,0:T(8,128)(2,1)S(1)}, u32[]{:S(2)}, u32[]{:S(2)}) collective-permute-start(bf16[2,128,128]{2,1,0:T(8,128)(2,1)S(1)} %get-tuple-element.145), channel_id=1, source_target_pairs={{4,0},{8,4},{12,8},{16,12},{20,16},{24,20},{28,24},{32,28},{36,32}... | collective-permute-start | bytes 196616 | tf_op jit(solution)/shard_map/ppermute | solution.py:26
  24.1 1.0 copy-start.10
  25.2 0.8 copy-start.11
  29.8 1.0 copy-start.10
  30.9 0.8 copy-start.11
  34.0 8.8 %copy-start.7 = (bf16[512,2048]{1,0:T(8,128)(2,1)}, bf16[512,2048]{1,0:T(8,128)(2,1)S(1)}, u32[]{:S(2)}) copy-start(bf16[512,2048]{1,0:T(8,128)(2,1)S(1)} %convolution_convert_fusion.1) | copy-start | bytes 6291460
  34.1 7.4 %collective-permute-start.2 = (bf16[64,2048]{1,0:T(8,128)(2,1)S(1)}, bf16[64,2048]{1,0:T(8,128)(2,1)S(1)}, u32[]{:S(2)}, u32[]{:S(2)}) collective-permute-start(bf16[64,2048]{1,0:T(8,128)(2,1)S(1)} %get-tuple-element.140), channel_id=1, source_target_pairs={{0,1},{1,2},{2,3},{3,0},{4,5},{5,6},{6,7},{7,4},{8,9},{9,10},{10,1... | collective-permute-start | bytes 786440 | tf_op jit(solution)/shard_map/ppermute | solution.py:66
  35.4 6.4 %collective-permute-start.4 = (bf16[64,2048]{1,0:T(8,128)(2,1)S(1)}, bf16[64,2048]{1,0:T(8,128)(2,1)S(1)}, u32[]{:S(2)}, u32[]{:S(2)}) collective-permute-start(bf16[64,2048]{1,0:T(8,128)(2,1)S(1)} %get-tuple-element.142), channel_id=1, source_target_pairs={{0,3},{1,0},{2,1},{3,2},{4,7},{5,4},{6,5},{7,6},{8,11},{9,8},{10,9... | collective-permute-start | bytes 786440 | tf_op jit(solution)/shard_map/ppermute | solution.py:66
  42.8 13.9 %collective-permute-start.5 = (bf16[128,2048]{1,0:T(8,128)(2,1)}, bf16[128,2048]{1,0:T(8,128)(2,1)S(1)}, u32[]{:S(2)}, u32[]{:S(2)}) collective-permute-start(bf16[128,2048]{1,0:T(8,128)(2,1)} %pad_maximum_fusion.1), channel_id=1, source_target_pairs={{0,3},{1,0},{2,1},{3,2},{4,7},{5,4},{6,5},{7,6},{8,11},{9,8},{10,9... | collective-permute-start | bytes 1572872 | tf_op jit(solution)/shard_map/ppermute | solution.py:66
  45.4 17.1 %copy-start.9 = (f32[2048]{0:T(1024)S(1)}, f32[2048]{0:T(1024)}, u32[]{:S(2)}) copy-start(f32[2048]{0:T(1024)} %param.17) | copy-start | bytes 24580
  46.2 14.6 %collective-permute-start.3 = (bf16[128,2048]{1,0:T(8,128)(2,1)}, bf16[128,2048]{1,0:T(8,128)(2,1)S(1)}, u32[]{:S(2)}, u32[]{:S(2)}) collective-permute-start(bf16[128,2048]{1,0:T(8,128)(2,1)} %pad_maximum_fusion), channel_id=1, source_target_pairs={{0,1},{1,2},{2,3},{3,0},{4,5},{5,6},{6,7},{7,4},{8,9},{9,10},{10,1... | collective-permute-start | bytes 1572872 | tf_op jit(solution)/shard_map/ppermute | solution.py:66
  62.4 23.1 %copy-start.5 = (f32[128,2048]{1,0:T(8,128)}, f32[128,2048]{1,0:T(8,128)S(1)}, u32[]{:S(2)}) copy-start(f32[128,2048]{1,0:T(8,128)S(1)} %get-tuple-element.131) | copy-start | bytes 3145732
  62.6 14.6 %collective-permute-start.7 = (bf16[128,2048]{1,0:T(8,128)(2,1)S(1)}, bf16[128,2048]{1,0:T(8,128)(2,1)S(1)}, u32[]{:S(2)}, u32[]{:S(2)}) collective-permute-start(bf16[128,2048]{1,0:T(8,128)(2,1)S(1)} %multiply_convert_fusion.own), channel_id=1, source_target_pairs={{0,1},{1,2},{2,3},{3,0},{4,5},{5,6},{6,7},{7,4},{8,9},{9,10},{10,1... | collective-permute-start | bytes 1572872 | tf_op jit(solution)/shard_map/ppermute | solution.py:66
  62.7 14.6 %collective-permute-start.6 = (bf16[128,2048]{1,0:T(8,128)(2,1)S(1)}, bf16[128,2048]{1,0:T(8,128)(2,1)S(1)}, u32[]{:S(2)}, u32[]{:S(2)}) collective-permute-start(bf16[128,2048]{1,0:T(8,128)(2,1)S(1)} %multiply_convert_fusion.own), channel_id=1, source_target_pairs={{0,3},{1,0},{2,1},{3,2},{4,7},{5,4},{6,5},{7,6},{8,11},{9,8},{10,9... | collective-permute-start | bytes 1572872 | tf_op jit(solution)/shard_map/ppermute | solution.py:66
  77.3 8.2 %collective-permute-start.8 = (bf16[64,2048]{1,0:T(8,128)(2,1)S(1)}, bf16[64,2048]{1,0:T(8,128)(2,1)S(1)}, u32[]{:S(2)}, u32[]{:S(2)}) collective-permute-start(bf16[64,2048]{1,0:T(8,128)(2,1)S(1)} %slice.70), channel_id=1, source_target_pairs={{0,1},{1,2},{2,3},{3,0},{4,5},{5,6},{6,7},{7,4},{8,9},{9,10},{10,1... | collective-permute-start | bytes 786440 | tf_op jit(solution)/shard_map/ppermute | solution.py:66
  77.4 0.8 copy-start.1
  78.2 7.3 %collective-permute-start.9 = (bf16[64,2048]{1,0:T(8,128)(2,1)S(1)}, bf16[64,2048]{1,0:T(8,128)(2,1)S(1)}, u32[]{:S(2)}, u32[]{:S(2)}) collective-permute-start(bf16[64,2048]{1,0:T(8,128)(2,1)S(1)} %slice.71), channel_id=1, source_target_pairs={{0,3},{1,0},{2,1},{3,2},{4,7},{5,4},{6,5},{7,6},{8,11},{9,8},{10,9... | collective-permute-start | bytes 786440 | tf_op jit(solution)/shard_map/ppermute | solution.py:66
  85.5 0.7 copy-start.3
  114.8 1.0 copy-start.2
  115.9 0.9 copy-start.4
  130.6 21.4 %copy-start.6 = (f32[128,2048]{1,0:T(8,128)S(1)}, f32[128,2048]{1,0:T(8,128)}, u32[]{:S(2)}) copy-start(f32[128,2048]{1,0:T(8,128)} %copy-done.5) | copy-start | bytes 3145732
  130.6 8.9 %collective-permute-start.10 = (bf16[64,2048]{1,0:T(8,128)(2,1)S(1)}, bf16[64,2048]{1,0:T(8,128)(2,1)S(1)}, u32[]{:S(2)}, u32[]{:S(2)}) collective-permute-start(bf16[64,2048]{1,0:T(8,128)(2,1)S(1)} %get-tuple-element.104), channel_id=1, source_target_pairs={{0,1},{1,2},{2,3},{3,0},{4,5},{5,6},{6,7},{7,4},{8,9},{9,10},{10,1... | collective-permute-start | bytes 786440 | tf_op jit(solution)/shard_map/ppermute | solution.py:66
  131.9 15.8 %collective-permute-start.12 = (bf16[64,2048]{1,0:T(8,128)(2,1)S(1)}, bf16[64,2048]{1,0:T(8,128)(2,1)S(1)}, u32[]{:S(2)}, u32[]{:S(2)}) collective-permute-start(bf16[64,2048]{1,0:T(8,128)(2,1)S(1)} %get-tuple-element.105), channel_id=1, source_target_pairs={{0,3},{1,0},{2,1},{3,2},{4,7},{5,4},{6,5},{7,6},{8,11},{9,8},{10,9... | collective-permute-start | bytes 786440 | tf_op jit(solution)/shard_map/ppermute | solution.py:66
  133.4 17.4 %collective-permute-start.13 = (bf16[64,2048]{1,0:T(8,128)(2,1)S(1)}, bf16[64,2048]{1,0:T(8,128)(2,1)S(1)}, u32[]{:S(2)}, u32[]{:S(2)}) collective-permute-start(bf16[64,2048]{1,0:T(8,128)(2,1)S(1)} %get-tuple-element.106), channel_id=1, source_target_pairs={{0,1},{1,2},{2,3},{3,0},{4,5},{5,6},{6,7},{7,4},{8,9},{9,10},{10,1... | collective-permute-start | bytes 786440 | tf_op jit(solution)/shard_map/ppermute | solution.py:66
  133.4 11.5 %collective-permute-start.14 = (bf16[64,2048]{1,0:T(8,128)(2,1)S(1)}, bf16[64,2048]{1,0:T(8,128)(2,1)S(1)}, u32[]{:S(2)}, u32[]{:S(2)}) collective-permute-start(bf16[64,2048]{1,0:T(8,128)(2,1)S(1)} %get-tuple-element.108), channel_id=1, source_target_pairs={{0,3},{1,0},{2,1},{3,2},{4,7},{5,4},{6,5},{7,6},{8,11},{9,8},{10,9... | collective-permute-start | bytes 786440 | tf_op jit(solution)/shard_map/ppermute | solution.py:66
  139.6 11.2 %collective-permute-start.11 = (bf16[64,2048]{1,0:T(8,128)(2,1)S(1)}, bf16[64,2048]{1,0:T(8,128)(2,1)S(1)}, u32[]{:S(2)}, u32[]{:S(2)}) collective-permute-start(bf16[64,2048]{1,0:T(8,128)(2,1)S(1)} %add_convert_fusion.1), channel_id=1, source_target_pairs={{0,1},{1,2},{2,3},{3,0},{4,5},{5,6},{6,7},{7,4},{8,9},{9,10},{10,1... | collective-permute-start | bytes 786440 | tf_op jit(solution)/shard_map/ppermute | solution.py:66
  144.9 7.0 %collective-permute-start.15 = (bf16[64,2048]{1,0:T(8,128)(2,1)S(1)}, bf16[64,2048]{1,0:T(8,128)(2,1)S(1)}, u32[]{:S(2)}, u32[]{:S(2)}) collective-permute-start(bf16[64,2048]{1,0:T(8,128)(2,1)S(1)} %add_convert_fusion), channel_id=1, source_target_pairs={{0,3},{1,0},{2,1},{3,2},{4,7},{5,4},{6,5},{7,6},{8,11},{9,8},{10,9... | collective-permute-start | bytes 786440 | tf_op jit(solution)/shard_map/ppermute | solution.py:66
Sparse Core Ops, SparseCore 0:
  10.1 104.7 all-gather.1

commit v3 on v2

--- a/solution.py
+++ b/solution.py
@@ -85,41 +85,54 @@
 
 
 FF_LOCAL = 1408
+LIMIT = 30
 STEPS = ((0, 256), (256, 256), (512, 256), (768, 256), (1024, 256), (1280, 128))
 
 
-def ffn_kernel(own, nxt, far_lo, far_hi, prv, w, *refs):
-    outs, mine, (hidden, wg, wd, sems) = refs[:6], refs[6], refs[7:]
-
-    def fetch(part, first, width, to, sem):
-        src = w.at[:, pl.ds(part * FF_LOCAL + first, width)]
-        return pltpu.make_async_copy(src, to, sem)
-
-    copies = []
+def ffn_rows(x, wg, wd, hidden, ready=None):
+    x = x[...]
     for n, (first, width) in enumerate(STEPS):
-        for part in range(2):
-            to = wg.at[:, pl.ds(2 * first + part * width, width)]
-            copies.append(fetch(part, first, width, to, sems.at[2 * n + part]))
-    downs = fetch(2, 0, FF_LOCAL, wd, sems.at[12])
-    for c in copies + [downs]:
-        c.start()
-    x = jnp.concatenate([far_lo[...], far_hi[...], nxt[...], prv[...], own[...]], axis=0)
-    for n, (first, width) in enumerate(STEPS):
-        copies[2 * n].wait()
-        copies[2 * n + 1].wait()
+        if ready is not None:
+            ready[2 * n].wait()
+            ready[2 * n + 1].wait()
         acc = jnp.dot(
             x, wg[:, 2 * first : 2 * (first + width)], preferred_element_type=jnp.float32
         )
         gate = acc[:, :width]
         hid = gate / (1.0 + jnp.exp(-gate)) * acc[:, width:]
         hidden[:, first : first + width] = hid.astype(jnp.bfloat16)
-    downs.wait()
-    res = lax.dot_general(
+    if ready is not None:
+        ready[12].wait()
+    return lax.dot_general(
         hidden[...], wd[...], (((1,), (1,)), ((), ())), preferred_element_type=jnp.float32
     )
+
+
+def first_kernel(x, w, *refs):
+    outs, (wg, wd, hidden, sems) = refs[:4], refs[4:]
+
+    def fetch(part, first, width, to, sem):
+        src = w.at[:, pl.ds(part * FF_LOCAL + first, width)]
+        return pltpu.make_async_copy(src, to, sem)
+
+    copies = []
+    for n, (first, width) in enumerate(STEPS):
+        for part in range(2):
+            to = wg.at[:, pl.ds(2 * first + part * width, width)]
+            copies.append(fetch(part, first, width, to, sems.at[2 * n + part]))
+    copies.append(fetch(2, 0, FF_LOCAL, wd, sems.at[12]))
+    for c in copies:
+        c.start()
+    res = ffn_rows(x, wg, wd, hidden, copies)
     for i, out in enumerate(outs):
         out[...] = res[64 * i : 64 * i + 64].astype(jnp.bfloat16)
-    mine[...] = res[384:]
+
+
+def second_kernel(x, wg, wd, nxt_out, prv_out, own_out, hidden):
+    res = ffn_rows(x, wg, wd, hidden)
+    nxt_out[...] = res[:64].astype(jnp.bfloat16)
+    prv_out[...] = res[64:128].astype(jnp.bfloat16)
+    own_out[...] = res[128:]
 
 
 def bf16(*shape):
@@ -129,22 +142,31 @@
 def feed_forward(own, nxt, far_lo, far_hi, prv, weights):
     vmem = pl.BlockSpec(memory_space=pltpu.VMEM)
     hbm = pl.BlockSpec(memory_space=pltpu.HBM)
-    out_lo, out_hi, nxt_lo, nxt_hi, prv_lo, prv_hi, mine = pl.pallas_call(
-        ffn_kernel,
-        out_shape=(bf16(64, 2048),) * 6 + (jax.ShapeDtypeStruct((128, 2048), jnp.float32),),
-        in_specs=[vmem] * 5 + [hbm],
-        out_specs=(vmem,) * 7,
-        scratch_shapes=[
-            pltpu.VMEM((512, FF_LOCAL), jnp.bfloat16),
-            pltpu.VMEM((2048, 2 * FF_LOCAL), jnp.bfloat16),
-            pltpu.VMEM((2048, FF_LOCAL), jnp.bfloat16),
-            pltpu.SemaphoreType.DMA((13,)),
-        ],
-        compiler_params=pltpu.CompilerParams(vmem_limit_bytes=36 * 1024 * 1024),
-        name="ffn",
-    )(own, nxt, far_lo, far_hi, prv, weights)
+    half = bf16(64, 2048)
+    x1 = jnp.concatenate([far_lo, far_hi, nxt[64:], prv[:64]])
+    x2 = jnp.concatenate([nxt[:64], prv[64:], own])
+    hidden = pltpu.VMEM((256, FF_LOCAL), jnp.bfloat16)
+    limit = pltpu.CompilerParams(vmem_limit_bytes=LIMIT * 1024 * 1024)
+    out_lo, out_hi, nxt_hi, prv_lo, wg, wd = pl.pallas_call(
+        first_kernel,
+        out_shape=(half,) * 4 + (bf16(2048, 2 * FF_LOCAL), bf16(2048, FF_LOCAL)),
+        in_specs=[vmem, hbm],
+        out_specs=(vmem,) * 6,
+        scratch_shapes=[hidden, pltpu.SemaphoreType.DMA((13,))],
+        compiler_params=limit,
+        name="ffn1",
+    )(x1, weights)
     up, down = hop(out_lo, 1), hop(out_hi, -1)
     prev_hi, next_lo = hop(nxt_hi, 1), hop(prv_lo, -1)
+    nxt_lo, prv_hi, mine = pl.pallas_call(
+        second_kernel,
+        out_shape=(half, half, jax.ShapeDtypeStruct((128, 2048), jnp.float32)),
+        in_specs=[vmem] * 3,
+        out_specs=(vmem,) * 3,
+        scratch_shapes=[hidden],
+        compiler_params=limit,
+        name="ffn2",
+    )(x2, wg, wd)
     up_sum = (nxt_lo.astype(jnp.float32) + up.astype(jnp.float32)).astype(jnp.bfloat16)
     down_sum = (prv_hi.astype(jnp.float32) + down.astype(jnp.float32)).astype(jnp.bfloat16)
     prev_lo, next_hi = hop(up_sum, 1), hop(down_sum, -1)

time: 162 us -> 156 us (0.963)
  waiting for transfers between devices: 81 us -> 75.9 us
  local copies, waits for them, and re-layouts: 9.84 us -> 7.58 us
    ppermute x14, waiting for transfers between devices: 48.8 us -> 44.1 us  [hop(): lax.ppermute(value, 'tp', [(i, (i + step) % size) for i in range(size)])]
    unnamed x20 -> x14, local copies, waits for them, and re-layouts: 3.52 us -> 1.25 us
    pallas_call x1 -> x2, Pallas kernels: 13.8 us -> 13.9 us  [the longest x1 8.55 us: feed_forward(): pl.pallas_call(first_kernel, out_shape=(half,) * 4 + (bf16(2048, 2 * FF_L...]
  transfers between devices with their start and end apart: 17 -> 17, of which waited for: 12 -> 11; matrix products, arithmetic and copies ran while one was open for 10% -> 11% of each run, Pallas kernels for 0% -> 3%
where the time goes in v3:
time: 156 us; the launch traced here: 154 us
  waiting for transfers between devices  75.9 us (49%)
  starting transfers between devices  25.8 us (17%)
  Pallas kernels  13.9 us (9%)
  between operations  13.7 us (9%)
  other arithmetic  11.2 us (7%)
  local copies, waits for them, and re-layouts  7.58 us (5%)
  matrix products  4.33 us (3%)
    ppermute x14, waiting for transfers between devices, hop(): lax.ppermute(value, 'tp', [(i, (i + step) % size) for i in range(size)])  44.1 us
    all_gather x1, waiting for transfers between devices, shards(): lax.all_gather(jnp.concatenate([gate_weight, up_weight, down_weight.T], a...  28.2 us
    ppermute x14, starting transfers between devices, hop(): lax.ppermute(value, 'tp', [(i, (i + step) % size) for i in range(size)])  19.4 us
    pallas_call x1, Pallas kernels, feed_forward(): pl.pallas_call(first_kernel, out_shape=(half,) * 4 + (bf16(2048, 2 * FF_L...  8.55 us
    pallas_call x1, Pallas kernels, feed_forward(): pl.pallas_call(second_kernel, out_shape=(half, half, jax.ShapeDtypeStruct...  5.35 us
    ppermute x1, starting transfers between devices, with_halo(): lax.ppermute(tail, axis, [(i, (i + 1) % count) for i in range(ends)])  4.5 us
    ppermute x1, waiting for transfers between devices, with_halo(): lax.ppermute(head, axis, [((i + 1) % count, i) for i in range(ends)])  3.57 us
  transfers between devices with their start and end apart: 17, of which 11 were waited for; matrix products, arithmetic and copies ran while one was open for 11% of the time, Pallas kernels for 3%

profile of v3, /device:TPU:1, one launch (start us, length us, event | category | flops | bytes accessed | tf_op | source)
XLA Modules:
  0.0 153.8 jit_solution(4009425381845628866)
XLA Ops:
  6.5 1.9 %pad_maximum_fusion.5 = bf16[32,4224]{1,0:T(8,128)(2,1)} fusion(bf16[32,1408]{1,0:T(8,128)(2,1)} %bitcast.78, bf16[32,1408]{1,0:T(8,128)(2,1)} %param.20, bf16[32,1408]{1,0:T(8,128)(2,1)} %param.19), kind=kLoop, calls=%fused_computation.45 | loop fusion | flops 811008 | bytes 540672 | tf_op jit(solution)/shard_map/concatenate | solution.py:224
  8.4 0.8 pad_maximum_fusion.7
  9.2 4.5 %collective-permute-start = (bf16[2,128,128]{2,1,0:T(8,128)(2,1)S(1)}, bf16[2,128,128]{2,1,0:T(8,128)(2,1)S(1)}, u32[]{:S(2)}, u32[]{:S(2)}) collective-permute-start(bf16[2,128,128]{2,1,0:T(8,128)(2,1)S(1)} %get-tuple-element.152), channel_id=1, source_target_pairs={{0,4},{4,8},{8,12},{12,16},{16,20},{20,24},{24,28},{28,32},{32,36}... | collective-permute-start | bytes 196616 | tf_op jit(solution)/shard_map/ppermute | solution.py:24
  13.8 1.9 %collective-permute-start.1 = (bf16[2,128,128]{2,1,0:T(8,128)(2,1)S(1)}, bf16[2,128,128]{2,1,0:T(8,128)(2,1)S(1)}, u32[]{:S(2)}, u32[]{:S(2)}) collective-permute-start(bf16[2,128,128]{2,1,0:T(8,128)(2,1)S(1)} %get-tuple-element.153), channel_id=1, source_target_pairs={{4,0},{8,4},{12,8},{16,12},{20,16},{24,20},{28,24},{32,28},{36,32}... | collective-permute-start | bytes 196616 | tf_op jit(solution)/shard_map/ppermute | solution.py:26
  15.8 3.6 %collective-permute-done.1 = bf16[2,128,128]{2,1,0:T(8,128)(2,1)S(1)} collective-permute-done((bf16[2,128,128]{2,1,0:T(8,128)(2,1)S(1)}, bf16[2,128,128]{2,1,0:T(8,128)(2,1)S(1)}, u32[]{:S(2)}, u32[]{:S(2)}) %collective-permute-start.1) | collective-permute-done | bytes 65568 | tf_op jit(solution)/shard_map/ppermute | solution.py:26
  19.3 1.0 pad_maximum_fusion.4
  20.4 11.1 %while.12 = (s32[]{:T(128)}, bf16[2,256,512]{2,1,0:T(8,128)(2,1)}, bf16[2,768,128]{2,1,0:T(8,128)(2,1)S(1)}, s32[2]{0:T(128)S(1)}, s32[]{:T(128)}, /*index=5*/bf...) while((s32[]{:T(128)}, bf16[2,256,512]{2,1,0:T(8,128)(2,1)}, ...), condition=%wide.region_3.4_spmd, body=%wide.region_0.3_spmd.sunk | while | flops 273420544 | bytes 14467428 | solution.py:207
  20.4 0.7 dynamic_slice.62
  22.0 1.0 constant_dynamic-slice_fusion.2
  23.1 0.5 fusion.40
  24.1 0.5 convolution_convert_fusion.3
  24.8 0.4 copy-done.7
  25.2 0.8 copy-done.8
  25.9 0.6 dynamic_slice.62
  27.5 1.0 constant_dynamic-slice_fusion.2
  28.7 0.5 fusion.40
  29.3 0.3 fusion.41
  29.6 0.5 convolution_convert_fusion.3
  30.3 0.4 copy-done.7
  30.7 0.8 copy-done.8
  31.5 2.3 %convolution_convert_fusion.1 = bf16[512,2048]{1,0:T(8,128)(2,1)S(1)} fusion(bf16[512,512]{1,0:T(8,128)(2,1)} %bitcast.79, bf16[512,2048]{1,0:T(8,128)(2,1)S(1)} %copy-done), kind=kOutput, calls=%fused_computation.23 | convolution fusion | flops 1074790400 | bytes 4718592 | tf_op jit(solution)/shard_map/dot_general | solution.py:212
  33.9 1.4 collective-permute-start.2
  35.3 1.5 %collective-permute-start.4 = (bf16[64,2048]{1,0:T(8,128)(2,1)S(1)}, bf16[64,2048]{1,0:T(8,128)(2,1)S(1)}, u32[]{:S(2)}, u32[]{:S(2)}) collective-permute-start(bf16[64,2048]{1,0:T(8,128)(2,1)S(1)} %get-tuple-element.146), channel_id=1, source_target_pairs={{0,3},{1,0},{2,1},{3,2},{4,7},{5,4},{6,5},{7,6},{8,11},{9,8},{10,9... | collective-permute-start | bytes 786440 | tf_op jit(solution)/shard_map/ppermute | solution.py:66
  36.8 4.5 %collective-permute-done.2 = bf16[64,2048]{1,0:T(8,128)(2,1)S(1)} collective-permute-done((bf16[64,2048]{1,0:T(8,128)(2,1)S(1)}, bf16[64,2048]{1,0:T(8,128)(2,1)S(1)}, u32[]{:S(2)}, u32[]{:S(2)}) %collective-permute-start.2) | collective-permute-done | bytes 262176 | tf_op jit(solution)/shard_map/ppermute | solution.py:66
  41.3 0.4 collective-permute-done.4
  41.8 0.8 pad_maximum_fusion.3
  42.6 2.6 %collective-permute-start.5 = (bf16[128,2048]{1,0:T(8,128)(2,1)}, bf16[128,2048]{1,0:T(8,128)(2,1)S(1)}, u32[]{:S(2)}, u32[]{:S(2)}) collective-permute-start(bf16[128,2048]{1,0:T(8,128)(2,1)} %pad_maximum_fusion.3), channel_id=1, source_target_pairs={{0,3},{1,0},{2,1},{3,2},{4,7},{5,4},{6,5},{7,6},{8,11},{9,8},{10,9... | collective-permute-start | bytes 1572872 | tf_op jit(solution)/shard_map/ppermute | solution.py:66
  45.2 0.8 pad_maximum_fusion.2
  46.1 10.5 %collective-permute-done.5 = bf16[128,2048]{1,0:T(8,128)(2,1)S(1)} collective-permute-done((bf16[128,2048]{1,0:T(8,128)(2,1)}, bf16[128,2048]{1,0:T(8,128)(2,1)S(1)}, u32[]{:S(2)}, u32[]{:S(2)}) %collective-permute-start.5) | collective-permute-done | bytes 524320 | tf_op jit(solution)/shard_map/ppermute | solution.py:66
  56.6 4.1 %collective-permute-done.3 = bf16[128,2048]{1,0:T(8,128)(2,1)S(1)} collective-permute-done((bf16[128,2048]{1,0:T(8,128)(2,1)}, bf16[128,2048]{1,0:T(8,128)(2,1)S(1)}, u32[]{:S(2)}, u32[]{:S(2)}) %collective-permute-start.3) | collective-permute-done | bytes 524320 | tf_op jit(solution)/shard_map/ppermute | solution.py:66
  60.7 1.6 %multiply_reduce_fusion = (f32[128]{0:T(128)S(1)}, f32[128,2048]{1,0:T(8,128)S(1)}) fusion(bf16[128,2048]{1,0:T(8,128)(2,1)S(1)} %collective-permute-done.5, bf16[128,2048]{1,0:T(8,128)(2,1)S(1)} %collective-permute-done.3, bf16[4,128,2048]{2,1,0:T(8,128)(2,1)} %bitcast.73, s32[]{:T(128)S(6)} %select_n.52, bf16[512,2048]{1,0:T(8,128)(2,1)} %param.16, ...), kind=kLoop, calls=%fused_computation.33 | loop fusion | flops 2359168 | bytes 3146248 | tf_op jit(solution)/shard_map/reduce_sum | solution.py:60
  62.6 2.7 %collective-permute-start.6 = (bf16[128,2048]{1,0:T(8,128)(2,1)S(1)}, bf16[128,2048]{1,0:T(8,128)(2,1)S(1)}, u32[]{:S(2)}, u32[]{:S(2)}) collective-permute-start(bf16[128,2048]{1,0:T(8,128)(2,1)S(1)} %multiply_convert_fusion), channel_id=1, source_target_pairs={{0,3},{1,0},{2,1},{3,2},{4,7},{5,4},{6,5},{7,6},{8,11},{9,8},{10,9... | collective-permute-start | bytes 1572872 | tf_op jit(solution)/shard_map/ppermute | solution.py:66
  65.3 11.8 %collective-permute-done.7 = bf16[128,2048]{1,0:T(8,128)(2,1)S(1)} collective-permute-done((bf16[128,2048]{1,0:T(8,128)(2,1)S(1)}, bf16[128,2048]{1,0:T(8,128)(2,1)S(1)}, u32[]{:S(2)}, u32[]{:S(2)}) %collective-permute-start.7) | collective-permute-done | bytes 524320 | tf_op jit(solution)/shard_map/ppermute | solution.py:66
  77.3 2.9 %collective-permute-start.9 = (bf16[64,2048]{1,0:T(8,128)(2,1)S(1)}, bf16[64,2048]{1,0:T(8,128)(2,1)S(1)}, u32[]{:S(2)}, u32[]{:S(2)}) collective-permute-start(bf16[64,2048]{1,0:T(8,128)(2,1)S(1)} %get-tuple-element.148), channel_id=1, source_target_pairs={{0,3},{1,0},{2,1},{3,2},{4,7},{5,4},{6,5},{7,6},{8,11},{9,8},{10,9... | collective-permute-start | bytes 786440 | tf_op jit(solution)/shard_map/ppermute | solution.py:66
  80.2 5.2 %collective-permute-done.8 = bf16[64,2048]{1,0:T(8,128)(2,1)S(1)} collective-permute-done((bf16[64,2048]{1,0:T(8,128)(2,1)S(1)}, bf16[64,2048]{1,0:T(8,128)(2,1)S(1)}, u32[]{:S(2)}, u32[]{:S(2)}) %collective-permute-start.8) | collective-permute-done | bytes 262176 | tf_op jit(solution)/shard_map/ppermute | solution.py:66
  85.4 1.2 pad_maximum_fusion
  86.6 28.2 %all-gather.2.cloned.1.call-done.w = bf16[2048,4224]{1,0:T(8,128)(2,1)} async-done(((bf16[32,4224]{1,0:T(8,128)(2,1)}), bf16[2048,4224]{1,0:T(8,128)(2,1)}) %all-gather.2.cloned.1.call-update) | async-done | bytes 17301520 | tf_op jit(solution)/shard_map/all_gather | solution.py:223
  114.8 1.2 copy-done.1
  116.0 8.5 %ffn1.1 = (bf16[64,2048]{1,0:T(8,128)(2,1)S(1)}, bf16[64,2048]{1,0:T(8,128)(2,1)S(1)}, bf16[64,2048]{1,0:T(8,128)(2,1)S(1)}, bf16[64,2048]{1,0:T(8,128)(2,1)S(1)...) custom-call(bf16[256,2048]{1,0:T(8,128)(2,1)S(1)} %copy-done.1, ...), custom_call_target="tpu_custom_call" | custom-call | tf_op jit(solution)/shard_map/ffn1/pallas_call | solution.py:150
  124.6 1.4 collective-permute-start.10
  126.0 1.3 collective-permute-start.12
  127.4 2.6 %collective-permute-start.14 = (bf16[64,2048]{1,0:T(8,128)(2,1)S(1)}, bf16[64,2048]{1,0:T(8,128)(2,1)S(1)}, u32[]{:S(2)}, u32[]{:S(2)}) collective-permute-start(bf16[64,2048]{1,0:T(8,128)(2,1)S(1)} %get-tuple-element.112), channel_id=1, source_target_pairs={{0,3},{1,0},{2,1},{3,2},{4,7},{5,4},{6,5},{7,6},{8,11},{9,8},{10,9... | collective-permute-start | bytes 786440 | tf_op jit(solution)/shard_map/ppermute | solution.py:66
  130.0 5.3 %ffn2.1 = (bf16[64,2048]{1,0:T(8,128)(2,1)S(1)}, bf16[64,2048]{1,0:T(8,128)(2,1)S(1)}, f32[128,2048]{1,0:T(8,128)S(1)}) custom-call(bf16[256,2048]{1,0:T(8,128)(2,1)S(1)} %get-tuple-element.154.x, bf16[2048,2816]{1,0:T(8,128)(2,1)S(1)} %get-tuple-element.104.wg, bf16[2048,1408]{1,0:T(8,128)(2,1)S(1)} %get-tuple-element.105.wd), custom_call_target="tpu_custom_call" | custom-call | tf_op jit(solution)/shard_map/ffn2/pallas_call | solution.py:161
  135.5 3.4 %collective-permute-done.14 = bf16[64,2048]{1,0:T(8,128)(2,1)S(1)} collective-permute-done((bf16[64,2048]{1,0:T(8,128)(2,1)S(1)}, bf16[64,2048]{1,0:T(8,128)(2,1)S(1)}, u32[]{:S(2)}, u32[]{:S(2)}) %collective-permute-start.14) | collective-permute-done | bytes 262176 | tf_op jit(solution)/shard_map/ppermute | solution.py:66
  139.0 2.6 %collective-permute-start.15 = (bf16[64,2048]{1,0:T(8,128)(2,1)S(1)}, bf16[64,2048]{1,0:T(8,128)(2,1)S(1)}, u32[]{:S(2)}, u32[]{:S(2)}) collective-permute-start(bf16[64,2048]{1,0:T(8,128)(2,1)S(1)} %add_convert_fusion), channel_id=1, source_target_pairs={{0,3},{1,0},{2,1},{3,2},{4,7},{5,4},{6,5},{7,6},{8,11},{9,8},{10,9... | collective-permute-start | bytes 786440 | tf_op jit(solution)/shard_map/ppermute | solution.py:66
  141.6 2.3 %collective-permute-done.11 = bf16[64,2048]{1,0:T(8,128)(2,1)S(1)} collective-permute-done((bf16[64,2048]{1,0:T(8,128)(2,1)S(1)}, bf16[64,2048]{1,0:T(8,128)(2,1)S(1)}, u32[]{:S(2)}, u32[]{:S(2)}) %collective-permute-start.11) | collective-permute-done | bytes 262176 | tf_op jit(solution)/shard_map/ppermute | solution.py:66
  144.0 1.9 %collective-permute-done.15 = bf16[64,2048]{1,0:T(8,128)(2,1)S(1)} collective-permute-done((bf16[64,2048]{1,0:T(8,128)(2,1)S(1)}, bf16[64,2048]{1,0:T(8,128)(2,1)S(1)}, u32[]{:S(2)}, u32[]{:S(2)}) %collective-permute-start.15) | collective-permute-done | bytes 262176 | tf_op jit(solution)/shard_map/ppermute | solution.py:66
  146.0 1.0 fusion.13
  (63 shorter events, 3.0 us)
Async XLA Ops:
  6.5 25.0 %copy-start = (bf16[512,2048]{1,0:T(8,128)(2,1)S(1)}, bf16[512,2048]{1,0:T(8,128)(2,1)}, u32[]{:S(2)}) copy-start(bf16[512,2048]{1,0:T(8,128)(2,1)} %param.18) | copy-start | bytes 6291460
  6.5 13.8 %copy-start.5 = (f32[4]{0:T(128)S(1)}, f32[4]{0:T(128)}, u32[]{:S(2)}) copy-start(f32[4]{0:T(128)} %param.15) | copy-start | bytes 52
  6.5 108.2 %all-gather.2.cloned.1.call-start = ((), (), s32[]{:S(2)}) async-start(), calls=%async_computation | async-start | bytes 17571840 | tf_op jit(solution)/shard_map/all_gather | solution.py:223
  9.2 6.5 %collective-permute-start = (bf16[2,128,128]{2,1,0:T(8,128)(2,1)S(1)}, bf16[2,128,128]{2,1,0:T(8,128)(2,1)S(1)}, u32[]{:S(2)}, u32[]{:S(2)}) collective-permute-start(bf16[2,128,128]{2,1,0:T(8,128)(2,1)S(1)} %get-tuple-element.152), channel_id=1, source_target_pairs={{0,4},{4,8},{8,12},{12,16},{16,20},{20,24},{24,28},{28,32},{32,36}... | collective-permute-start | bytes 196616 | tf_op jit(solution)/shard_map/ppermute | solution.py:24
  13.8 5.6 %collective-permute-start.1 = (bf16[2,128,128]{2,1,0:T(8,128)(2,1)S(1)}, bf16[2,128,128]{2,1,0:T(8,128)(2,1)S(1)}, u32[]{:S(2)}, u32[]{:S(2)}) collective-permute-start(bf16[2,128,128]{2,1,0:T(8,128)(2,1)S(1)} %get-tuple-element.153), channel_id=1, source_target_pairs={{4,0},{8,4},{12,8},{16,12},{20,16},{24,20},{28,24},{32,28},{36,32}... | collective-permute-start | bytes 196616 | tf_op jit(solution)/shard_map/ppermute | solution.py:26
  24.1 1.0 copy-start.7
  25.1 0.8 copy-start.8
  29.6 1.0 copy-start.7
  30.7 0.8 copy-start.8
  33.8 8.8 %copy-start.4 = (bf16[512,2048]{1,0:T(8,128)(2,1)}, bf16[512,2048]{1,0:T(8,128)(2,1)S(1)}, u32[]{:S(2)}) copy-start(bf16[512,2048]{1,0:T(8,128)(2,1)S(1)} %convolution_convert_fusion.1) | copy-start | bytes 6291460
  33.9 7.4 %collective-permute-start.2 = (bf16[64,2048]{1,0:T(8,128)(2,1)S(1)}, bf16[64,2048]{1,0:T(8,128)(2,1)S(1)}, u32[]{:S(2)}, u32[]{:S(2)}) collective-permute-start(bf16[64,2048]{1,0:T(8,128)(2,1)S(1)} %get-tuple-element.144), channel_id=1, source_target_pairs={{0,1},{1,2},{2,3},{3,0},{4,5},{5,6},{6,7},{7,4},{8,9},{9,10},{10,1... | collective-permute-start | bytes 786440 | tf_op jit(solution)/shard_map/ppermute | solution.py:66
  35.3 6.4 %collective-permute-start.4 = (bf16[64,2048]{1,0:T(8,128)(2,1)S(1)}, bf16[64,2048]{1,0:T(8,128)(2,1)S(1)}, u32[]{:S(2)}, u32[]{:S(2)}) collective-permute-start(bf16[64,2048]{1,0:T(8,128)(2,1)S(1)} %get-tuple-element.146), channel_id=1, source_target_pairs={{0,3},{1,0},{2,1},{3,2},{4,7},{5,4},{6,5},{7,6},{8,11},{9,8},{10,9... | collective-permute-start | bytes 786440 | tf_op jit(solution)/shard_map/ppermute | solution.py:66
  42.6 14.0 %collective-permute-start.5 = (bf16[128,2048]{1,0:T(8,128)(2,1)}, bf16[128,2048]{1,0:T(8,128)(2,1)S(1)}, u32[]{:S(2)}, u32[]{:S(2)}) collective-permute-start(bf16[128,2048]{1,0:T(8,128)(2,1)} %pad_maximum_fusion.3), channel_id=1, source_target_pairs={{0,3},{1,0},{2,1},{3,2},{4,7},{5,4},{6,5},{7,6},{8,11},{9,8},{10,9... | collective-permute-start | bytes 1572872 | tf_op jit(solution)/shard_map/ppermute | solution.py:66
  45.2 17.1 %copy-start.6 = (f32[2048]{0:T(1024)S(1)}, f32[2048]{0:T(1024)}, u32[]{:S(2)}) copy-start(f32[2048]{0:T(1024)} %param.17) | copy-start | bytes 24580
  46.1 14.7 %collective-permute-start.3 = (bf16[128,2048]{1,0:T(8,128)(2,1)}, bf16[128,2048]{1,0:T(8,128)(2,1)S(1)}, u32[]{:S(2)}, u32[]{:S(2)}) collective-permute-start(bf16[128,2048]{1,0:T(8,128)(2,1)} %pad_maximum_fusion.2), channel_id=1, source_target_pairs={{0,1},{1,2},{2,3},{3,0},{4,5},{5,6},{6,7},{7,4},{8,9},{9,10},{10,1... | collective-permute-start | bytes 1572872 | tf_op jit(solution)/shard_map/ppermute | solution.py:66
  62.3 23.1 %copy-start.2 = (f32[128,2048]{1,0:T(8,128)}, f32[128,2048]{1,0:T(8,128)S(1)}, u32[]{:S(2)}) copy-start(f32[128,2048]{1,0:T(8,128)S(1)} %get-tuple-element.135) | copy-start | bytes 3145732
  62.5 14.6 %collective-permute-start.7 = (bf16[128,2048]{1,0:T(8,128)(2,1)S(1)}, bf16[128,2048]{1,0:T(8,128)(2,1)S(1)}, u32[]{:S(2)}, u32[]{:S(2)}) collective-permute-start(bf16[128,2048]{1,0:T(8,128)(2,1)S(1)} %multiply_convert_fusion), channel_id=1, source_target_pairs={{0,1},{1,2},{2,3},{3,0},{4,5},{5,6},{6,7},{7,4},{8,9},{9,10},{10,1... | collective-permute-start | bytes 1572872 | tf_op jit(solution)/shard_map/ppermute | solution.py:66
  62.6 14.6 %collective-permute-start.6 = (bf16[128,2048]{1,0:T(8,128)(2,1)S(1)}, bf16[128,2048]{1,0:T(8,128)(2,1)S(1)}, u32[]{:S(2)}, u32[]{:S(2)}) collective-permute-start(bf16[128,2048]{1,0:T(8,128)(2,1)S(1)} %multiply_convert_fusion), channel_id=1, source_target_pairs={{0,3},{1,0},{2,1},{3,2},{4,7},{5,4},{6,5},{7,6},{8,11},{9,8},{10,9... | collective-permute-start | bytes 1572872 | tf_op jit(solution)/shard_map/ppermute | solution.py:66
  77.2 8.2 %collective-permute-start.8 = (bf16[64,2048]{1,0:T(8,128)(2,1)S(1)}, bf16[64,2048]{1,0:T(8,128)(2,1)S(1)}, u32[]{:S(2)}, u32[]{:S(2)}) collective-permute-start(bf16[64,2048]{1,0:T(8,128)(2,1)S(1)} %get-tuple-element.150), channel_id=1, source_target_pairs={{0,1},{1,2},{2,3},{3,0},{4,5},{5,6},{6,7},{7,4},{8,9},{9,10},{10,1... | collective-permute-start | bytes 786440 | tf_op jit(solution)/shard_map/ppermute | solution.py:66
  77.3 8.1 %collective-permute-start.9 = (bf16[64,2048]{1,0:T(8,128)(2,1)S(1)}, bf16[64,2048]{1,0:T(8,128)(2,1)S(1)}, u32[]{:S(2)}, u32[]{:S(2)}) collective-permute-start(bf16[64,2048]{1,0:T(8,128)(2,1)S(1)} %get-tuple-element.148), channel_id=1, source_target_pairs={{0,3},{1,0},{2,1},{3,2},{4,7},{5,4},{6,5},{7,6},{8,11},{9,8},{10,9... | collective-permute-start | bytes 786440 | tf_op jit(solution)/shard_map/ppermute | solution.py:66
  114.8 1.2 copy-start.1
  124.6 10.8 %collective-permute-start.10 = (bf16[64,2048]{1,0:T(8,128)(2,1)S(1)}, bf16[64,2048]{1,0:T(8,128)(2,1)S(1)}, u32[]{:S(2)}, u32[]{:S(2)}) collective-permute-start(bf16[64,2048]{1,0:T(8,128)(2,1)S(1)} %get-tuple-element.108), channel_id=1, source_target_pairs={{0,1},{1,2},{2,3},{3,0},{4,5},{5,6},{6,7},{7,4},{8,9},{9,10},{10,1... | collective-permute-start | bytes 786440 | tf_op jit(solution)/shard_map/ppermute | solution.py:66
  126.0 15.6 %collective-permute-start.12 = (bf16[64,2048]{1,0:T(8,128)(2,1)S(1)}, bf16[64,2048]{1,0:T(8,128)(2,1)S(1)}, u32[]{:S(2)}, u32[]{:S(2)}) collective-permute-start(bf16[64,2048]{1,0:T(8,128)(2,1)S(1)} %get-tuple-element.109), channel_id=1, source_target_pairs={{0,3},{1,0},{2,1},{3,2},{4,7},{5,4},{6,5},{7,6},{8,11},{9,8},{10,9... | collective-permute-start | bytes 786440 | tf_op jit(solution)/shard_map/ppermute | solution.py:66
  127.3 16.7 %collective-permute-start.13 = (bf16[64,2048]{1,0:T(8,128)(2,1)S(1)}, bf16[64,2048]{1,0:T(8,128)(2,1)S(1)}, u32[]{:S(2)}, u32[]{:S(2)}) collective-permute-start(bf16[64,2048]{1,0:T(8,128)(2,1)S(1)} %get-tuple-element.110), channel_id=1, source_target_pairs={{0,1},{1,2},{2,3},{3,0},{4,5},{5,6},{6,7},{7,4},{8,9},{9,10},{10,1... | collective-permute-start | bytes 786440 | tf_op jit(solution)/shard_map/ppermute | solution.py:66
  127.4 11.5 %collective-permute-start.14 = (bf16[64,2048]{1,0:T(8,128)(2,1)S(1)}, bf16[64,2048]{1,0:T(8,128)(2,1)S(1)}, u32[]{:S(2)}, u32[]{:S(2)}) collective-permute-start(bf16[64,2048]{1,0:T(8,128)(2,1)S(1)} %get-tuple-element.112), channel_id=1, source_target_pairs={{0,3},{1,0},{2,1},{3,2},{4,7},{5,4},{6,5},{7,6},{8,11},{9,8},{10,9... | collective-permute-start | bytes 786440 | tf_op jit(solution)/shard_map/ppermute | solution.py:66
  135.4 10.6 %copy-start.3 = (f32[128,2048]{1,0:T(8,128)S(1)}, f32[128,2048]{1,0:T(8,128)}, u32[]{:S(2)}) copy-start(f32[128,2048]{1,0:T(8,128)} %copy-done.2) | copy-start | bytes 3145732
  135.4 8.5 %collective-permute-start.11 = (bf16[64,2048]{1,0:T(8,128)(2,1)S(1)}, bf16[64,2048]{1,0:T(8,128)(2,1)S(1)}, u32[]{:S(2)}, u32[]{:S(2)}) collective-permute-start(bf16[64,2048]{1,0:T(8,128)(2,1)S(1)} %add_convert_fusion.1), channel_id=1, source_target_pairs={{0,1},{1,2},{2,3},{3,0},{4,5},{5,6},{6,7},{7,4},{8,9},{9,10},{10,1... | collective-permute-start | bytes 786440 | tf_op jit(solution)/shard_map/ppermute | solution.py:66
  139.0 6.9 %collective-permute-start.15 = (bf16[64,2048]{1,0:T(8,128)(2,1)S(1)}, bf16[64,2048]{1,0:T(8,128)(2,1)S(1)}, u32[]{:S(2)}, u32[]{:S(2)}) collective-permute-start(bf16[64,2048]{1,0:T(8,128)(2,1)S(1)} %add_convert_fusion), channel_id=1, source_target_pairs={{0,3},{1,0},{2,1},{3,2},{4,7},{5,4},{6,5},{7,6},{8,11},{9,8},{10,9... | collective-permute-start | bytes 786440 | tf_op jit(solution)/shard_map/ppermute | solution.py:66
Sparse Core Ops, SparseCore 0:
  10.1 104.6 all-gather.1

commit v4 on v3

--- a/solution.py
+++ b/solution.py
@@ -4,6 +4,7 @@
 from jax.experimental import pallas as pl
 from jax.experimental.pallas import tpu as pltpu
 from jax.sharding import PartitionSpec as P
+
 
 DH = 128
 WIN = 128
@@ -156,8 +157,10 @@
         compiler_params=limit,
         name="ffn1",
     )(x1, weights)
-    up, down = hop(out_lo, 1), hop(out_hi, -1)
-    prev_hi, next_lo = hop(nxt_hi, 1), hop(prv_lo, -1)
+    up = hop(out_lo, 1)
+    down = hop(out_hi, -1)
+    prev_hi = hop(nxt_hi, 1)
+    next_lo = hop(prv_lo, -1)
     nxt_lo, prv_hi, mine = pl.pallas_call(
         second_kernel,
         out_shape=(half, half, jax.ShapeDtypeStruct((128, 2048), jnp.float32)),

time: 156 us -> 156 us (level)
  no operation moved by 1% of the time
where the time goes in v4:
time: 156 us; the launch traced here: 154 us
  waiting for transfers between devices  75.9 us (49%)
  starting transfers between devices  25.8 us (17%)
  Pallas kernels  13.9 us (9%)
  between operations  13.7 us (9%)
  other arithmetic  11.2 us (7%)
  local copies, waits for them, and re-layouts  7.58 us (5%)
  matrix products  4.33 us (3%)
    ppermute x14, waiting for transfers between devices, hop(): lax.ppermute(value, 'tp', [(i, (i + step) % size) for i in range(size)])  44.1 us
    all_gather x1, waiting for transfers between devices, shards(): lax.all_gather(jnp.concatenate([gate_weight, up_weight, down_weight.T], a...  28.2 us
    ppermute x14, starting transfers between devices, hop(): lax.ppermute(value, 'tp', [(i, (i + step) % size) for i in range(size)])  19.4 us
    pallas_call x1, Pallas kernels, feed_forward(): pl.pallas_call(first_kernel, out_shape=(half,) * 4 + (bf16(2048, 2 * FF_L...  8.55 us
    pallas_call x1, Pallas kernels, feed_forward(): pl.pallas_call(second_kernel, out_shape=(half, half, jax.ShapeDtypeStruct...  5.35 us
    ppermute x1, starting transfers between devices, with_halo(): lax.ppermute(tail, axis, [(i, (i + 1) % count) for i in range(ends)])  4.5 us
    ppermute x1, waiting for transfers between devices, with_halo(): lax.ppermute(head, axis, [((i + 1) % count, i) for i in range(ends)])  3.57 us
  transfers between devices with their start and end apart: 17, of which 11 were waited for; matrix products, arithmetic and copies ran while one was open for 11% of the time, Pallas kernels for 3%

profile of v4, /device:TPU:1, one launch (start us, length us, event | category | flops | bytes accessed | tf_op | source)
XLA Modules:
  0.0 153.8 jit_solution(4009425381845628866)
XLA Ops:
  6.5 1.9 %pad_maximum_fusion.5 = bf16[32,4224]{1,0:T(8,128)(2,1)} fusion(bf16[32,1408]{1,0:T(8,128)(2,1)} %bitcast.78, bf16[32,1408]{1,0:T(8,128)(2,1)} %param.20, bf16[32,1408]{1,0:T(8,128)(2,1)} %param.19), kind=kLoop, calls=%fused_computation.45 | loop fusion | flops 811008 | bytes 540672 | tf_op jit(solution)/shard_map/concatenate | solution.py:227
  8.4 0.8 pad_maximum_fusion.7
  9.2 4.5 %collective-permute-start = (bf16[2,128,128]{2,1,0:T(8,128)(2,1)S(1)}, bf16[2,128,128]{2,1,0:T(8,128)(2,1)S(1)}, u32[]{:S(2)}, u32[]{:S(2)}) collective-permute-start(bf16[2,128,128]{2,1,0:T(8,128)(2,1)S(1)} %get-tuple-element.152), channel_id=1, source_target_pairs={{0,4},{4,8},{8,12},{12,16},{16,20},{20,24},{24,28},{28,32},{32,36}... | collective-permute-start | bytes 196616 | tf_op jit(solution)/shard_map/ppermute | solution.py:25
  13.8 1.9 %collective-permute-start.1 = (bf16[2,128,128]{2,1,0:T(8,128)(2,1)S(1)}, bf16[2,128,128]{2,1,0:T(8,128)(2,1)S(1)}, u32[]{:S(2)}, u32[]{:S(2)}) collective-permute-start(bf16[2,128,128]{2,1,0:T(8,128)(2,1)S(1)} %get-tuple-element.153), channel_id=1, source_target_pairs={{4,0},{8,4},{12,8},{16,12},{20,16},{24,20},{28,24},{32,28},{36,32}... | collective-permute-start | bytes 196616 | tf_op jit(solution)/shard_map/ppermute | solution.py:27
  15.8 3.6 %collective-permute-done.1 = bf16[2,128,128]{2,1,0:T(8,128)(2,1)S(1)} collective-permute-done((bf16[2,128,128]{2,1,0:T(8,128)(2,1)S(1)}, bf16[2,128,128]{2,1,0:T(8,128)(2,1)S(1)}, u32[]{:S(2)}, u32[]{:S(2)}) %collective-permute-start.1) | collective-permute-done | bytes 65568 | tf_op jit(solution)/shard_map/ppermute | solution.py:27
  19.3 1.0 pad_maximum_fusion.4
  20.4 11.1 %while.12 = (s32[]{:T(128)}, bf16[2,256,512]{2,1,0:T(8,128)(2,1)}, bf16[2,768,128]{2,1,0:T(8,128)(2,1)S(1)}, s32[2]{0:T(128)S(1)}, s32[]{:T(128)}, /*index=5*/bf...) while((s32[]{:T(128)}, bf16[2,256,512]{2,1,0:T(8,128)(2,1)}, ...), condition=%wide.region_3.4_spmd, body=%wide.region_0.3_spmd.sunk | while | flops 273420544 | bytes 14467428 | solution.py:210
  20.4 0.7 dynamic_slice.62
  22.0 1.0 constant_dynamic-slice_fusion.2
  23.1 0.5 fusion.40
  24.1 0.5 convolution_convert_fusion.3
  24.8 0.4 copy-done.7
  25.2 0.8 copy-done.8
  25.9 0.6 dynamic_slice.62
  27.5 1.0 constant_dynamic-slice_fusion.2
  28.7 0.5 fusion.40
  29.3 0.3 fusion.41
  29.6 0.5 convolution_convert_fusion.3
  30.3 0.4 copy-done.7
  30.7 0.8 copy-done.8
  31.5 2.3 %convolution_convert_fusion.1 = bf16[512,2048]{1,0:T(8,128)(2,1)S(1)} fusion(bf16[512,512]{1,0:T(8,128)(2,1)} %bitcast.79, bf16[512,2048]{1,0:T(8,128)(2,1)S(1)} %copy-done), kind=kOutput, calls=%fused_computation.23 | convolution fusion | flops 1074790400 | bytes 4718592 | tf_op jit(solution)/shard_map/dot_general | solution.py:215
  33.9 1.4 collective-permute-start.2
  35.3 1.5 %collective-permute-start.4 = (bf16[64,2048]{1,0:T(8,128)(2,1)S(1)}, bf16[64,2048]{1,0:T(8,128)(2,1)S(1)}, u32[]{:S(2)}, u32[]{:S(2)}) collective-permute-start(bf16[64,2048]{1,0:T(8,128)(2,1)S(1)} %get-tuple-element.146), channel_id=1, source_target_pairs={{0,3},{1,0},{2,1},{3,2},{4,7},{5,4},{6,5},{7,6},{8,11},{9,8},{10,9... | collective-permute-start | bytes 786440 | tf_op jit(solution)/shard_map/ppermute | solution.py:67
  36.8 4.5 %collective-permute-done.2 = bf16[64,2048]{1,0:T(8,128)(2,1)S(1)} collective-permute-done((bf16[64,2048]{1,0:T(8,128)(2,1)S(1)}, bf16[64,2048]{1,0:T(8,128)(2,1)S(1)}, u32[]{:S(2)}, u32[]{:S(2)}) %collective-permute-start.2) | collective-permute-done | bytes 262176 | tf_op jit(solution)/shard_map/ppermute | solution.py:67
  41.3 0.4 collective-permute-done.4
  41.8 0.8 pad_maximum_fusion.3
  42.6 2.6 %collective-permute-start.5 = (bf16[128,2048]{1,0:T(8,128)(2,1)}, bf16[128,2048]{1,0:T(8,128)(2,1)S(1)}, u32[]{:S(2)}, u32[]{:S(2)}) collective-permute-start(bf16[128,2048]{1,0:T(8,128)(2,1)} %pad_maximum_fusion.3), channel_id=1, source_target_pairs={{0,3},{1,0},{2,1},{3,2},{4,7},{5,4},{6,5},{7,6},{8,11},{9,8},{10,9... | collective-permute-start | bytes 1572872 | tf_op jit(solution)/shard_map/ppermute | solution.py:67
  45.2 0.8 pad_maximum_fusion.2
  46.1 10.5 %collective-permute-done.5 = bf16[128,2048]{1,0:T(8,128)(2,1)S(1)} collective-permute-done((bf16[128,2048]{1,0:T(8,128)(2,1)}, bf16[128,2048]{1,0:T(8,128)(2,1)S(1)}, u32[]{:S(2)}, u32[]{:S(2)}) %collective-permute-start.5) | collective-permute-done | bytes 524320 | tf_op jit(solution)/shard_map/ppermute | solution.py:67
  56.6 4.1 %collective-permute-done.3 = bf16[128,2048]{1,0:T(8,128)(2,1)S(1)} collective-permute-done((bf16[128,2048]{1,0:T(8,128)(2,1)}, bf16[128,2048]{1,0:T(8,128)(2,1)S(1)}, u32[]{:S(2)}, u32[]{:S(2)}) %collective-permute-start.3) | collective-permute-done | bytes 524320 | tf_op jit(solution)/shard_map/ppermute | solution.py:67
  60.7 1.6 %multiply_reduce_fusion = (f32[128]{0:T(128)S(1)}, f32[128,2048]{1,0:T(8,128)S(1)}) fusion(bf16[128,2048]{1,0:T(8,128)(2,1)S(1)} %collective-permute-done.5, bf16[128,2048]{1,0:T(8,128)(2,1)S(1)} %collective-permute-done.3, bf16[4,128,2048]{2,1,0:T(8,128)(2,1)} %bitcast.73, s32[]{:T(128)S(6)} %select_n.52, bf16[512,2048]{1,0:T(8,128)(2,1)} %param.16, ...), kind=kLoop, calls=%fused_computation.33 | loop fusion | flops 2359168 | bytes 3146248 | tf_op jit(solution)/shard_map/reduce_sum | solution.py:61
  62.6 2.7 %collective-permute-start.6 = (bf16[128,2048]{1,0:T(8,128)(2,1)S(1)}, bf16[128,2048]{1,0:T(8,128)(2,1)S(1)}, u32[]{:S(2)}, u32[]{:S(2)}) collective-permute-start(bf16[128,2048]{1,0:T(8,128)(2,1)S(1)} %multiply_convert_fusion), channel_id=1, source_target_pairs={{0,3},{1,0},{2,1},{3,2},{4,7},{5,4},{6,5},{7,6},{8,11},{9,8},{10,9... | collective-permute-start | bytes 1572872 | tf_op jit(solution)/shard_map/ppermute | solution.py:67
  65.3 11.8 %collective-permute-done.7 = bf16[128,2048]{1,0:T(8,128)(2,1)S(1)} collective-permute-done((bf16[128,2048]{1,0:T(8,128)(2,1)S(1)}, bf16[128,2048]{1,0:T(8,128)(2,1)S(1)}, u32[]{:S(2)}, u32[]{:S(2)}) %collective-permute-start.7) | collective-permute-done | bytes 524320 | tf_op jit(solution)/shard_map/ppermute | solution.py:67
  77.3 2.9 %collective-permute-start.9 = (bf16[64,2048]{1,0:T(8,128)(2,1)S(1)}, bf16[64,2048]{1,0:T(8,128)(2,1)S(1)}, u32[]{:S(2)}, u32[]{:S(2)}) collective-permute-start(bf16[64,2048]{1,0:T(8,128)(2,1)S(1)} %get-tuple-element.148), channel_id=1, source_target_pairs={{0,3},{1,0},{2,1},{3,2},{4,7},{5,4},{6,5},{7,6},{8,11},{9,8},{10,9... | collective-permute-start | bytes 786440 | tf_op jit(solution)/shard_map/ppermute | solution.py:67
  80.2 5.2 %collective-permute-done.8 = bf16[64,2048]{1,0:T(8,128)(2,1)S(1)} collective-permute-done((bf16[64,2048]{1,0:T(8,128)(2,1)S(1)}, bf16[64,2048]{1,0:T(8,128)(2,1)S(1)}, u32[]{:S(2)}, u32[]{:S(2)}) %collective-permute-start.8) | collective-permute-done | bytes 262176 | tf_op jit(solution)/shard_map/ppermute | solution.py:67
  85.4 1.2 pad_maximum_fusion
  86.6 28.2 %all-gather.2.cloned.1.call-done.w = bf16[2048,4224]{1,0:T(8,128)(2,1)} async-done(((bf16[32,4224]{1,0:T(8,128)(2,1)}), bf16[2048,4224]{1,0:T(8,128)(2,1)}) %all-gather.2.cloned.1.call-update) | async-done | bytes 17301520 | tf_op jit(solution)/shard_map/all_gather | solution.py:226
  114.8 1.2 copy-done.1
  116.0 8.5 %ffn1.1 = (bf16[64,2048]{1,0:T(8,128)(2,1)S(1)}, bf16[64,2048]{1,0:T(8,128)(2,1)S(1)}, bf16[64,2048]{1,0:T(8,128)(2,1)S(1)}, bf16[64,2048]{1,0:T(8,128)(2,1)S(1)...) custom-call(bf16[256,2048]{1,0:T(8,128)(2,1)S(1)} %copy-done.1, ...), custom_call_target="tpu_custom_call" | custom-call | tf_op jit(solution)/shard_map/ffn1/pallas_call | solution.py:151
  124.6 1.4 collective-permute-start.10
  126.0 1.3 collective-permute-start.12
  127.4 2.6 %collective-permute-start.14 = (bf16[64,2048]{1,0:T(8,128)(2,1)S(1)}, bf16[64,2048]{1,0:T(8,128)(2,1)S(1)}, u32[]{:S(2)}, u32[]{:S(2)}) collective-permute-start(bf16[64,2048]{1,0:T(8,128)(2,1)S(1)} %get-tuple-element.112), channel_id=1, source_target_pairs={{0,3},{1,0},{2,1},{3,2},{4,7},{5,4},{6,5},{7,6},{8,11},{9,8},{10,9... | collective-permute-start | bytes 786440 | tf_op jit(solution)/shard_map/ppermute | solution.py:67
  130.0 5.3 %ffn2.1 = (bf16[64,2048]{1,0:T(8,128)(2,1)S(1)}, bf16[64,2048]{1,0:T(8,128)(2,1)S(1)}, f32[128,2048]{1,0:T(8,128)S(1)}) custom-call(bf16[256,2048]{1,0:T(8,128)(2,1)S(1)} %get-tuple-element.154.x, bf16[2048,2816]{1,0:T(8,128)(2,1)S(1)} %get-tuple-element.104.wg, bf16[2048,1408]{1,0:T(8,128)(2,1)S(1)} %get-tuple-element.105.wd), custom_call_target="tpu_custom_call" | custom-call | tf_op jit(solution)/shard_map/ffn2/pallas_call | solution.py:164
  135.5 3.4 %collective-permute-done.14 = bf16[64,2048]{1,0:T(8,128)(2,1)S(1)} collective-permute-done((bf16[64,2048]{1,0:T(8,128)(2,1)S(1)}, bf16[64,2048]{1,0:T(8,128)(2,1)S(1)}, u32[]{:S(2)}, u32[]{:S(2)}) %collective-permute-start.14) | collective-permute-done | bytes 262176 | tf_op jit(solution)/shard_map/ppermute | solution.py:67
  139.0 2.6 %collective-permute-start.15 = (bf16[64,2048]{1,0:T(8,128)(2,1)S(1)}, bf16[64,2048]{1,0:T(8,128)(2,1)S(1)}, u32[]{:S(2)}, u32[]{:S(2)}) collective-permute-start(bf16[64,2048]{1,0:T(8,128)(2,1)S(1)} %add_convert_fusion), channel_id=1, source_target_pairs={{0,3},{1,0},{2,1},{3,2},{4,7},{5,4},{6,5},{7,6},{8,11},{9,8},{10,9... | collective-permute-start | bytes 786440 | tf_op jit(solution)/shard_map/ppermute | solution.py:67
  141.6 2.3 %collective-permute-done.11 = bf16[64,2048]{1,0:T(8,128)(2,1)S(1)} collective-permute-done((bf16[64,2048]{1,0:T(8,128)(2,1)S(1)}, bf16[64,2048]{1,0:T(8,128)(2,1)S(1)}, u32[]{:S(2)}, u32[]{:S(2)}) %collective-permute-start.11) | collective-permute-done | bytes 262176 | tf_op jit(solution)/shard_map/ppermute | solution.py:67
  144.0 1.9 %collective-permute-done.15 = bf16[64,2048]{1,0:T(8,128)(2,1)S(1)} collective-permute-done((bf16[64,2048]{1,0:T(8,128)(2,1)S(1)}, bf16[64,2048]{1,0:T(8,128)(2,1)S(1)}, u32[]{:S(2)}, u32[]{:S(2)}) %collective-permute-start.15) | collective-permute-done | bytes 262176 | tf_op jit(solution)/shard_map/ppermute | solution.py:67
  146.0 1.0 fusion.13
  (63 shorter events, 3.0 us)
Async XLA Ops:
  6.5 25.0 %copy-start = (bf16[512,2048]{1,0:T(8,128)(2,1)S(1)}, bf16[512,2048]{1,0:T(8,128)(2,1)}, u32[]{:S(2)}) copy-start(bf16[512,2048]{1,0:T(8,128)(2,1)} %param.18) | copy-start | bytes 6291460
  6.5 13.8 %copy-start.5 = (f32[4]{0:T(128)S(1)}, f32[4]{0:T(128)}, u32[]{:S(2)}) copy-start(f32[4]{0:T(128)} %param.15) | copy-start | bytes 52
  6.5 108.2 %all-gather.2.cloned.1.call-start = ((), (), s32[]{:S(2)}) async-start(), calls=%async_computation | async-start | bytes 17571840 | tf_op jit(solution)/shard_map/all_gather | solution.py:226
  9.2 6.5 %collective-permute-start = (bf16[2,128,128]{2,1,0:T(8,128)(2,1)S(1)}, bf16[2,128,128]{2,1,0:T(8,128)(2,1)S(1)}, u32[]{:S(2)}, u32[]{:S(2)}) collective-permute-start(bf16[2,128,128]{2,1,0:T(8,128)(2,1)S(1)} %get-tuple-element.152), channel_id=1, source_target_pairs={{0,4},{4,8},{8,12},{12,16},{16,20},{20,24},{24,28},{28,32},{32,36}... | collective-permute-start | bytes 196616 | tf_op jit(solution)/shard_map/ppermute | solution.py:25
  13.8 5.6 %collective-permute-start.1 = (bf16[2,128,128]{2,1,0:T(8,128)(2,1)S(1)}, bf16[2,128,128]{2,1,0:T(8,128)(2,1)S(1)}, u32[]{:S(2)}, u32[]{:S(2)}) collective-permute-start(bf16[2,128,128]{2,1,0:T(8,128)(2,1)S(1)} %get-tuple-element.153), channel_id=1, source_target_pairs={{4,0},{8,4},{12,8},{16,12},{20,16},{24,20},{28,24},{32,28},{36,32}... | collective-permute-start | bytes 196616 | tf_op jit(solution)/shard_map/ppermute | solution.py:27
  24.1 1.0 copy-start.7
  25.1 0.8 copy-start.8
  29.6 1.0 copy-start.7
  30.7 0.8 copy-start.8
  33.8 8.8 %copy-start.4 = (bf16[512,2048]{1,0:T(8,128)(2,1)}, bf16[512,2048]{1,0:T(8,128)(2,1)S(1)}, u32[]{:S(2)}) copy-start(bf16[512,2048]{1,0:T(8,128)(2,1)S(1)} %convolution_convert_fusion.1) | copy-start | bytes 6291460
  33.9 7.4 %collective-permute-start.2 = (bf16[64,2048]{1,0:T(8,128)(2,1)S(1)}, bf16[64,2048]{1,0:T(8,128)(2,1)S(1)}, u32[]{:S(2)}, u32[]{:S(2)}) collective-permute-start(bf16[64,2048]{1,0:T(8,128)(2,1)S(1)} %get-tuple-element.144), channel_id=1, source_target_pairs={{0,1},{1,2},{2,3},{3,0},{4,5},{5,6},{6,7},{7,4},{8,9},{9,10},{10,1... | collective-permute-start | bytes 786440 | tf_op jit(solution)/shard_map/ppermute | solution.py:67
  35.3 6.4 %collective-permute-start.4 = (bf16[64,2048]{1,0:T(8,128)(2,1)S(1)}, bf16[64,2048]{1,0:T(8,128)(2,1)S(1)}, u32[]{:S(2)}, u32[]{:S(2)}) collective-permute-start(bf16[64,2048]{1,0:T(8,128)(2,1)S(1)} %get-tuple-element.146), channel_id=1, source_target_pairs={{0,3},{1,0},{2,1},{3,2},{4,7},{5,4},{6,5},{7,6},{8,11},{9,8},{10,9... | collective-permute-start | bytes 786440 | tf_op jit(solution)/shard_map/ppermute | solution.py:67
  42.6 14.0 %collective-permute-start.5 = (bf16[128,2048]{1,0:T(8,128)(2,1)}, bf16[128,2048]{1,0:T(8,128)(2,1)S(1)}, u32[]{:S(2)}, u32[]{:S(2)}) collective-permute-start(bf16[128,2048]{1,0:T(8,128)(2,1)} %pad_maximum_fusion.3), channel_id=1, source_target_pairs={{0,3},{1,0},{2,1},{3,2},{4,7},{5,4},{6,5},{7,6},{8,11},{9,8},{10,9... | collective-permute-start | bytes 1572872 | tf_op jit(solution)/shard_map/ppermute | solution.py:67
  45.2 17.1 %copy-start.6 = (f32[2048]{0:T(1024)S(1)}, f32[2048]{0:T(1024)}, u32[]{:S(2)}) copy-start(f32[2048]{0:T(1024)} %param.17) | copy-start | bytes 24580
  46.1 14.7 %collective-permute-start.3 = (bf16[128,2048]{1,0:T(8,128)(2,1)}, bf16[128,2048]{1,0:T(8,128)(2,1)S(1)}, u32[]{:S(2)}, u32[]{:S(2)}) collective-permute-start(bf16[128,2048]{1,0:T(8,128)(2,1)} %pad_maximum_fusion.2), channel_id=1, source_target_pairs={{0,1},{1,2},{2,3},{3,0},{4,5},{5,6},{6,7},{7,4},{8,9},{9,10},{10,1... | collective-permute-start | bytes 1572872 | tf_op jit(solution)/shard_map/ppermute | solution.py:67
  62.3 23.1 %copy-start.2 = (f32[128,2048]{1,0:T(8,128)}, f32[128,2048]{1,0:T(8,128)S(1)}, u32[]{:S(2)}) copy-start(f32[128,2048]{1,0:T(8,128)S(1)} %get-tuple-element.135) | copy-start | bytes 3145732
  62.5 14.6 %collective-permute-start.7 = (bf16[128,2048]{1,0:T(8,128)(2,1)S(1)}, bf16[128,2048]{1,0:T(8,128)(2,1)S(1)}, u32[]{:S(2)}, u32[]{:S(2)}) collective-permute-start(bf16[128,2048]{1,0:T(8,128)(2,1)S(1)} %multiply_convert_fusion), channel_id=1, source_target_pairs={{0,1},{1,2},{2,3},{3,0},{4,5},{5,6},{6,7},{7,4},{8,9},{9,10},{10,1... | collective-permute-start | bytes 1572872 | tf_op jit(solution)/shard_map/ppermute | solution.py:67
  62.6 14.6 %collective-permute-start.6 = (bf16[128,2048]{1,0:T(8,128)(2,1)S(1)}, bf16[128,2048]{1,0:T(8,128)(2,1)S(1)}, u32[]{:S(2)}, u32[]{:S(2)}) collective-permute-start(bf16[128,2048]{1,0:T(8,128)(2,1)S(1)} %multiply_convert_fusion), channel_id=1, source_target_pairs={{0,3},{1,0},{2,1},{3,2},{4,7},{5,4},{6,5},{7,6},{8,11},{9,8},{10,9... | collective-permute-start | bytes 1572872 | tf_op jit(solution)/shard_map/ppermute | solution.py:67
  77.2 8.2 %collective-permute-start.8 = (bf16[64,2048]{1,0:T(8,128)(2,1)S(1)}, bf16[64,2048]{1,0:T(8,128)(2,1)S(1)}, u32[]{:S(2)}, u32[]{:S(2)}) collective-permute-start(bf16[64,2048]{1,0:T(8,128)(2,1)S(1)} %get-tuple-element.150), channel_id=1, source_target_pairs={{0,1},{1,2},{2,3},{3,0},{4,5},{5,6},{6,7},{7,4},{8,9},{9,10},{10,1... | collective-permute-start | bytes 786440 | tf_op jit(solution)/shard_map/ppermute | solution.py:67
  77.3 8.1 %collective-permute-start.9 = (bf16[64,2048]{1,0:T(8,128)(2,1)S(1)}, bf16[64,2048]{1,0:T(8,128)(2,1)S(1)}, u32[]{:S(2)}, u32[]{:S(2)}) collective-permute-start(bf16[64,2048]{1,0:T(8,128)(2,1)S(1)} %get-tuple-element.148), channel_id=1, source_target_pairs={{0,3},{1,0},{2,1},{3,2},{4,7},{5,4},{6,5},{7,6},{8,11},{9,8},{10,9... | collective-permute-start | bytes 786440 | tf_op jit(solution)/shard_map/ppermute | solution.py:67
  114.8 1.2 copy-start.1
  124.6 10.8 %collective-permute-start.10 = (bf16[64,2048]{1,0:T(8,128)(2,1)S(1)}, bf16[64,2048]{1,0:T(8,128)(2,1)S(1)}, u32[]{:S(2)}, u32[]{:S(2)}) collective-permute-start(bf16[64,2048]{1,0:T(8,128)(2,1)S(1)} %get-tuple-element.108), channel_id=1, source_target_pairs={{0,1},{1,2},{2,3},{3,0},{4,5},{5,6},{6,7},{7,4},{8,9},{9,10},{10,1... | collective-permute-start | bytes 786440 | tf_op jit(solution)/shard_map/ppermute | solution.py:67
  126.0 15.6 %collective-permute-start.12 = (bf16[64,2048]{1,0:T(8,128)(2,1)S(1)}, bf16[64,2048]{1,0:T(8,128)(2,1)S(1)}, u32[]{:S(2)}, u32[]{:S(2)}) collective-permute-start(bf16[64,2048]{1,0:T(8,128)(2,1)S(1)} %get-tuple-element.109), channel_id=1, source_target_pairs={{0,3},{1,0},{2,1},{3,2},{4,7},{5,4},{6,5},{7,6},{8,11},{9,8},{10,9... | collective-permute-start | bytes 786440 | tf_op jit(solution)/shard_map/ppermute | solution.py:67
  127.3 16.7 %collective-permute-start.13 = (bf16[64,2048]{1,0:T(8,128)(2,1)S(1)}, bf16[64,2048]{1,0:T(8,128)(2,1)S(1)}, u32[]{:S(2)}, u32[]{:S(2)}) collective-permute-start(bf16[64,2048]{1,0:T(8,128)(2,1)S(1)} %get-tuple-element.110), channel_id=1, source_target_pairs={{0,1},{1,2},{2,3},{3,0},{4,5},{5,6},{6,7},{7,4},{8,9},{9,10},{10,1... | collective-permute-start | bytes 786440 | tf_op jit(solution)/shard_map/ppermute | solution.py:67
  127.4 11.5 %collective-permute-start.14 = (bf16[64,2048]{1,0:T(8,128)(2,1)S(1)}, bf16[64,2048]{1,0:T(8,128)(2,1)S(1)}, u32[]{:S(2)}, u32[]{:S(2)}) collective-permute-start(bf16[64,2048]{1,0:T(8,128)(2,1)S(1)} %get-tuple-element.112), channel_id=1, source_target_pairs={{0,3},{1,0},{2,1},{3,2},{4,7},{5,4},{6,5},{7,6},{8,11},{9,8},{10,9... | collective-permute-start | bytes 786440 | tf_op jit(solution)/shard_map/ppermute | solution.py:67
  135.4 10.6 %copy-start.3 = (f32[128,2048]{1,0:T(8,128)S(1)}, f32[128,2048]{1,0:T(8,128)}, u32[]{:S(2)}) copy-start(f32[128,2048]{1,0:T(8,128)} %copy-done.2) | copy-start | bytes 3145732
  135.4 8.5 %collective-permute-start.11 = (bf16[64,2048]{1,0:T(8,128)(2,1)S(1)}, bf16[64,2048]{1,0:T(8,128)(2,1)S(1)}, u32[]{:S(2)}, u32[]{:S(2)}) collective-permute-start(bf16[64,2048]{1,0:T(8,128)(2,1)S(1)} %add_convert_fusion.1), channel_id=1, source_target_pairs={{0,1},{1,2},{2,3},{3,0},{4,5},{5,6},{6,7},{7,4},{8,9},{9,10},{10,1... | collective-permute-start | bytes 786440 | tf_op jit(solution)/shard_map/ppermute | solution.py:67
  139.0 6.9 %collective-permute-start.15 = (bf16[64,2048]{1,0:T(8,128)(2,1)S(1)}, bf16[64,2048]{1,0:T(8,128)(2,1)S(1)}, u32[]{:S(2)}, u32[]{:S(2)}) collective-permute-start(bf16[64,2048]{1,0:T(8,128)(2,1)S(1)} %add_convert_fusion), channel_id=1, source_target_pairs={{0,3},{1,0},{2,1},{3,2},{4,7},{5,4},{6,5},{7,6},{8,11},{9,8},{10,9... | collective-permute-start | bytes 786440 | tf_op jit(solution)/shard_map/ppermute | solution.py:67
Sparse Core Ops, SparseCore 0:
  10.1 104.6 all-gather.1

commit v5 on v4

--- a/solution.py
+++ b/solution.py
@@ -229,13 +229,9 @@
     mine, prev_lo, prev_hi, next_lo, next_hi = feed_forward(
         normed, nxt, far_lo, far_hi, prv, weights
     )
-    ffn_share = mine + jnp.concatenate(
-        [
-            prev_lo.astype(jnp.float32) + next_lo.astype(jnp.float32),
-            prev_hi.astype(jnp.float32) + next_hi.astype(jnp.float32),
-        ]
-    )
-    return (middle_own + ffn_share).astype(jnp.bfloat16)
+    ready = (middle_own + mine) + jnp.concatenate([next_lo, prev_hi]).astype(jnp.float32)
+    ready, prev_lo, next_hi = lax.optimization_barrier((ready, prev_lo, next_hi))
+    return (ready + jnp.concatenate([prev_lo, next_hi]).astype(jnp.float32)).astype(jnp.bfloat16)
 
 
 def solution(mesh):

time: 156 us -> 156 us (level)
  no operation moved by 1% of the time
where the time goes in v5:
time: 156 us; the launch traced here: 154 us
  waiting for transfers between devices  75.7 us (49%)
  starting transfers between devices  25.8 us (17%)
  Pallas kernels  13.9 us (9%)
  between operations  13.7 us (9%)
  other arithmetic  11.2 us (7%)
  local copies, waits for them, and re-layouts  7.58 us (5%)
  matrix products  4.33 us (3%)
    ppermute x14, waiting for transfers between devices, hop(): lax.ppermute(value, 'tp', [(i, (i + step) % size) for i in range(size)])  43.9 us
    all_gather x1, waiting for transfers between devices, shards(): lax.all_gather(jnp.concatenate([gate_weight, up_weight, down_weight.T], a...  28.2 us
    ppermute x14, starting transfers between devices, hop(): lax.ppermute(value, 'tp', [(i, (i + step) % size) for i in range(size)])  19.4 us
    pallas_call x1, Pallas kernels, feed_forward(): pl.pallas_call(first_kernel, out_shape=(half,) * 4 + (bf16(2048, 2 * FF_L...  8.55 us
    pallas_call x1, Pallas kernels, feed_forward(): pl.pallas_call(second_kernel, out_shape=(half, half, jax.ShapeDtypeStruct...  5.35 us
    ppermute x1, starting transfers between devices, with_halo(): lax.ppermute(tail, axis, [(i, (i + 1) % count) for i in range(ends)])  4.5 us
    ppermute x1, waiting for transfers between devices, with_halo(): lax.ppermute(head, axis, [((i + 1) % count, i) for i in range(ends)])  3.57 us
  transfers between devices with their start and end apart: 17, of which 11 were waited for; matrix products, arithmetic and copies ran while one was open for 11% of the time, Pallas kernels for 3%

profile of v5, /device:TPU:1, one launch (start us, length us, event | category | flops | bytes accessed | tf_op | source)
XLA Modules:
  0.0 153.6 jit_solution(14802215567157034253)
XLA Ops:
  6.5 1.9 %pad_maximum_fusion.5 = bf16[32,4224]{1,0:T(8,128)(2,1)} fusion(bf16[32,1408]{1,0:T(8,128)(2,1)} %bitcast.78, bf16[32,1408]{1,0:T(8,128)(2,1)} %param.20, bf16[32,1408]{1,0:T(8,128)(2,1)} %param.19), kind=kLoop, calls=%fused_computation.42 | loop fusion | flops 811008 | bytes 540672 | tf_op jit(solution)/shard_map/concatenate | solution.py:227
  8.4 0.8 pad_maximum_fusion.7
  9.2 4.5 %collective-permute-start = (bf16[2,128,128]{2,1,0:T(8,128)(2,1)S(1)}, bf16[2,128,128]{2,1,0:T(8,128)(2,1)S(1)}, u32[]{:S(2)}, u32[]{:S(2)}) collective-permute-start(bf16[2,128,128]{2,1,0:T(8,128)(2,1)S(1)} %get-tuple-element.158), channel_id=1, source_target_pairs={{0,4},{4,8},{8,12},{12,16},{16,20},{20,24},{24,28},{28,32},{32,36}... | collective-permute-start | bytes 196616 | tf_op jit(solution)/shard_map/ppermute | solution.py:25
  13.8 1.9 %collective-permute-start.1 = (bf16[2,128,128]{2,1,0:T(8,128)(2,1)S(1)}, bf16[2,128,128]{2,1,0:T(8,128)(2,1)S(1)}, u32[]{:S(2)}, u32[]{:S(2)}) collective-permute-start(bf16[2,128,128]{2,1,0:T(8,128)(2,1)S(1)} %get-tuple-element.159), channel_id=1, source_target_pairs={{4,0},{8,4},{12,8},{16,12},{20,16},{24,20},{28,24},{32,28},{36,32}... | collective-permute-start | bytes 196616 | tf_op jit(solution)/shard_map/ppermute | solution.py:27
  15.8 3.6 %collective-permute-done.1 = bf16[2,128,128]{2,1,0:T(8,128)(2,1)S(1)} collective-permute-done((bf16[2,128,128]{2,1,0:T(8,128)(2,1)S(1)}, bf16[2,128,128]{2,1,0:T(8,128)(2,1)S(1)}, u32[]{:S(2)}, u32[]{:S(2)}) %collective-permute-start.1) | collective-permute-done | bytes 65568 | tf_op jit(solution)/shard_map/ppermute | solution.py:27
  19.3 1.0 pad_maximum_fusion.4
  20.4 11.1 %while.12 = (s32[]{:T(128)}, bf16[2,256,512]{2,1,0:T(8,128)(2,1)}, bf16[2,768,128]{2,1,0:T(8,128)(2,1)S(1)}, s32[2]{0:T(128)S(1)}, s32[]{:T(128)}, /*index=5*/bf...) while((s32[]{:T(128)}, bf16[2,256,512]{2,1,0:T(8,128)(2,1)}, ...), condition=%wide.region_3.4_spmd, body=%wide.region_0.3_spmd.sunk | while | flops 273420544 | bytes 14467428 | solution.py:210
  20.4 0.7 dynamic_slice.62
  22.0 1.0 constant_dynamic-slice_fusion.2
  23.1 0.5 fusion.38
  24.1 0.5 convolution_convert_fusion.3
  24.8 0.4 copy-done.7
  25.2 0.8 copy-done.8
  25.9 0.6 dynamic_slice.62
  27.5 1.0 constant_dynamic-slice_fusion.2
  28.7 0.5 fusion.38
  29.3 0.3 fusion.39
  29.6 0.5 convolution_convert_fusion.3
  30.3 0.4 copy-done.7
  30.7 0.8 copy-done.8
  31.5 2.3 %convolution_convert_fusion.1 = bf16[512,2048]{1,0:T(8,128)(2,1)S(1)} fusion(bf16[512,512]{1,0:T(8,128)(2,1)} %bitcast.79, bf16[512,2048]{1,0:T(8,128)(2,1)S(1)} %copy-done), kind=kOutput, calls=%fused_computation.23 | convolution fusion | flops 1074790400 | bytes 4718592 | tf_op jit(solution)/shard_map/dot_general | solution.py:215
  33.9 1.4 collective-permute-start.2
  35.3 1.5 %collective-permute-start.4 = (bf16[64,2048]{1,0:T(8,128)(2,1)S(1)}, bf16[64,2048]{1,0:T(8,128)(2,1)S(1)}, u32[]{:S(2)}, u32[]{:S(2)}) collective-permute-start(bf16[64,2048]{1,0:T(8,128)(2,1)S(1)} %get-tuple-element.152), channel_id=1, source_target_pairs={{0,3},{1,0},{2,1},{3,2},{4,7},{5,4},{6,5},{7,6},{8,11},{9,8},{10,9... | collective-permute-start | bytes 786440 | tf_op jit(solution)/shard_map/ppermute | solution.py:67
  36.8 4.5 %collective-permute-done.2 = bf16[64,2048]{1,0:T(8,128)(2,1)S(1)} collective-permute-done((bf16[64,2048]{1,0:T(8,128)(2,1)S(1)}, bf16[64,2048]{1,0:T(8,128)(2,1)S(1)}, u32[]{:S(2)}, u32[]{:S(2)}) %collective-permute-start.2) | collective-permute-done | bytes 262176 | tf_op jit(solution)/shard_map/ppermute | solution.py:67
  41.3 0.4 collective-permute-done.4
  41.8 0.8 pad_maximum_fusion.3
  42.6 2.6 %collective-permute-start.5 = (bf16[128,2048]{1,0:T(8,128)(2,1)}, bf16[128,2048]{1,0:T(8,128)(2,1)S(1)}, u32[]{:S(2)}, u32[]{:S(2)}) collective-permute-start(bf16[128,2048]{1,0:T(8,128)(2,1)} %pad_maximum_fusion.3), channel_id=1, source_target_pairs={{0,3},{1,0},{2,1},{3,2},{4,7},{5,4},{6,5},{7,6},{8,11},{9,8},{10,9... | collective-permute-start | bytes 1572872 | tf_op jit(solution)/shard_map/ppermute | solution.py:67
  45.2 0.8 pad_maximum_fusion.2
  46.1 10.5 %collective-permute-done.5 = bf16[128,2048]{1,0:T(8,128)(2,1)S(1)} collective-permute-done((bf16[128,2048]{1,0:T(8,128)(2,1)}, bf16[128,2048]{1,0:T(8,128)(2,1)S(1)}, u32[]{:S(2)}, u32[]{:S(2)}) %collective-permute-start.5) | collective-permute-done | bytes 524320 | tf_op jit(solution)/shard_map/ppermute | solution.py:67
  56.6 4.1 %collective-permute-done.3 = bf16[128,2048]{1,0:T(8,128)(2,1)S(1)} collective-permute-done((bf16[128,2048]{1,0:T(8,128)(2,1)}, bf16[128,2048]{1,0:T(8,128)(2,1)S(1)}, u32[]{:S(2)}, u32[]{:S(2)}) %collective-permute-start.3) | collective-permute-done | bytes 524320 | tf_op jit(solution)/shard_map/ppermute | solution.py:67
  60.7 1.6 %multiply_reduce_fusion = (f32[128]{0:T(128)S(1)}, f32[128,2048]{1,0:T(8,128)S(1)}) fusion(bf16[128,2048]{1,0:T(8,128)(2,1)S(1)} %collective-permute-done.5, bf16[128,2048]{1,0:T(8,128)(2,1)S(1)} %collective-permute-done.3, bf16[4,128,2048]{2,1,0:T(8,128)(2,1)} %bitcast.73, s32[]{:T(128)S(6)} %select_n.52, bf16[512,2048]{1,0:T(8,128)(2,1)} %param.16, ...), kind=kLoop, calls=%fused_computation.32 | loop fusion | flops 2359168 | bytes 3146248 | tf_op jit(solution)/shard_map/reduce_sum | solution.py:61
  62.6 2.7 %collective-permute-start.6 = (bf16[128,2048]{1,0:T(8,128)(2,1)S(1)}, bf16[128,2048]{1,0:T(8,128)(2,1)S(1)}, u32[]{:S(2)}, u32[]{:S(2)}) collective-permute-start(bf16[128,2048]{1,0:T(8,128)(2,1)S(1)} %multiply_convert_fusion), channel_id=1, source_target_pairs={{0,3},{1,0},{2,1},{3,2},{4,7},{5,4},{6,5},{7,6},{8,11},{9,8},{10,9... | collective-permute-start | bytes 1572872 | tf_op jit(solution)/shard_map/ppermute | solution.py:67
  65.3 11.8 %collective-permute-done.7 = bf16[128,2048]{1,0:T(8,128)(2,1)S(1)} collective-permute-done((bf16[128,2048]{1,0:T(8,128)(2,1)S(1)}, bf16[128,2048]{1,0:T(8,128)(2,1)S(1)}, u32[]{:S(2)}, u32[]{:S(2)}) %collective-permute-start.7) | collective-permute-done | bytes 524320 | tf_op jit(solution)/shard_map/ppermute | solution.py:67
  77.3 2.9 %collective-permute-start.9 = (bf16[64,2048]{1,0:T(8,128)(2,1)S(1)}, bf16[64,2048]{1,0:T(8,128)(2,1)S(1)}, u32[]{:S(2)}, u32[]{:S(2)}) collective-permute-start(bf16[64,2048]{1,0:T(8,128)(2,1)S(1)} %get-tuple-element.154), channel_id=1, source_target_pairs={{0,3},{1,0},{2,1},{3,2},{4,7},{5,4},{6,5},{7,6},{8,11},{9,8},{10,9... | collective-permute-start | bytes 786440 | tf_op jit(solution)/shard_map/ppermute | solution.py:67
  80.2 5.2 %collective-permute-done.8 = bf16[64,2048]{1,0:T(8,128)(2,1)S(1)} collective-permute-done((bf16[64,2048]{1,0:T(8,128)(2,1)S(1)}, bf16[64,2048]{1,0:T(8,128)(2,1)S(1)}, u32[]{:S(2)}, u32[]{:S(2)}) %collective-permute-start.8) | collective-permute-done | bytes 262176 | tf_op jit(solution)/shard_map/ppermute | solution.py:67
  85.4 1.2 pad_maximum_fusion
  86.6 28.2 %all-gather.2.cloned.1.call-done.w = bf16[2048,4224]{1,0:T(8,128)(2,1)} async-done(((bf16[32,4224]{1,0:T(8,128)(2,1)}), bf16[2048,4224]{1,0:T(8,128)(2,1)}) %all-gather.2.cloned.1.call-update) | async-done | bytes 17301520 | tf_op jit(solution)/shard_map/all_gather | solution.py:226
  114.8 1.2 copy-done.1
  116.0 8.5 %ffn1.1 = (bf16[64,2048]{1,0:T(8,128)(2,1)S(1)}, bf16[64,2048]{1,0:T(8,128)(2,1)S(1)}, bf16[64,2048]{1,0:T(8,128)(2,1)S(1)}, bf16[64,2048]{1,0:T(8,128)(2,1)S(1)...) custom-call(bf16[256,2048]{1,0:T(8,128)(2,1)S(1)} %copy-done.1, ...), custom_call_target="tpu_custom_call" | custom-call | tf_op jit(solution)/shard_map/ffn1/pallas_call | solution.py:151
  124.6 1.4 collective-permute-start.12
  126.0 1.3 collective-permute-start.10
  127.4 2.6 %collective-permute-start.14 = (bf16[64,2048]{1,0:T(8,128)(2,1)S(1)}, bf16[64,2048]{1,0:T(8,128)(2,1)S(1)}, u32[]{:S(2)}, u32[]{:S(2)}) collective-permute-start(bf16[64,2048]{1,0:T(8,128)(2,1)S(1)} %get-tuple-element.115), channel_id=1, source_target_pairs={{0,3},{1,0},{2,1},{3,2},{4,7},{5,4},{6,5},{7,6},{8,11},{9,8},{10,9... | collective-permute-start | bytes 786440 | tf_op jit(solution)/shard_map/ppermute | solution.py:67
  130.0 5.3 %ffn2.1 = (bf16[64,2048]{1,0:T(8,128)(2,1)S(1)}, bf16[64,2048]{1,0:T(8,128)(2,1)S(1)}, f32[128,2048]{1,0:T(8,128)S(1)}) custom-call(bf16[256,2048]{1,0:T(8,128)(2,1)S(1)} %get-tuple-element.160.x, bf16[2048,2816]{1,0:T(8,128)(2,1)S(1)} %get-tuple-element.107.wg, bf16[2048,1408]{1,0:T(8,128)(2,1)S(1)} %get-tuple-element.108.wd), custom_call_target="tpu_custom_call" | custom-call | tf_op jit(solution)/shard_map/ffn2/pallas_call | solution.py:164
  135.5 3.4 %collective-permute-done.14 = bf16[64,2048]{1,0:T(8,128)(2,1)S(1)} collective-permute-done((bf16[64,2048]{1,0:T(8,128)(2,1)S(1)}, bf16[64,2048]{1,0:T(8,128)(2,1)S(1)}, u32[]{:S(2)}, u32[]{:S(2)}) %collective-permute-start.14) | collective-permute-done | bytes 262176 | tf_op jit(solution)/shard_map/ppermute | solution.py:67
  139.0 2.6 %collective-permute-start.15 = (bf16[64,2048]{1,0:T(8,128)(2,1)S(1)}, bf16[64,2048]{1,0:T(8,128)(2,1)S(1)}, u32[]{:S(2)}, u32[]{:S(2)}) collective-permute-start(bf16[64,2048]{1,0:T(8,128)(2,1)S(1)} %add_convert_fusion.1), channel_id=1, source_target_pairs={{0,3},{1,0},{2,1},{3,2},{4,7},{5,4},{6,5},{7,6},{8,11},{9,8},{10,9... | collective-permute-start | bytes 786440 | tf_op jit(solution)/shard_map/ppermute | solution.py:67
  141.8 2.1 %collective-permute-done.13 = bf16[64,2048]{1,0:T(8,128)(2,1)S(1)} collective-permute-done((bf16[64,2048]{1,0:T(8,128)(2,1)S(1)}, bf16[64,2048]{1,0:T(8,128)(2,1)S(1)}, u32[]{:S(2)}, u32[]{:S(2)}) %collective-permute-start.13) | collective-permute-done | bytes 262176 | tf_op jit(solution)/shard_map/ppermute | solution.py:67
  143.9 2.0 %collective-permute-done.15 = bf16[64,2048]{1,0:T(8,128)(2,1)S(1)} collective-permute-done((bf16[64,2048]{1,0:T(8,128)(2,1)S(1)}, bf16[64,2048]{1,0:T(8,128)(2,1)S(1)}, u32[]{:S(2)}, u32[]{:S(2)}) %collective-permute-start.15) | collective-permute-done | bytes 262176 | tf_op jit(solution)/shard_map/ppermute | solution.py:67
  145.9 0.9 add_convert_fusion
  (62 shorter events, 3.0 us)
Async XLA Ops:
  6.5 25.0 %copy-start = (bf16[512,2048]{1,0:T(8,128)(2,1)S(1)}, bf16[512,2048]{1,0:T(8,128)(2,1)}, u32[]{:S(2)}) copy-start(bf16[512,2048]{1,0:T(8,128)(2,1)} %param.18) | copy-start | bytes 6291460
  6.5 13.8 %copy-start.5 = (f32[4]{0:T(128)S(1)}, f32[4]{0:T(128)}, u32[]{:S(2)}) copy-start(f32[4]{0:T(128)} %param.15) | copy-start | bytes 52
  6.5 108.2 %all-gather.2.cloned.1.call-start = ((), (), s32[]{:S(2)}) async-start(), calls=%async_computation | async-start | bytes 17571840 | tf_op jit(solution)/shard_map/all_gather | solution.py:226
  9.2 6.5 %collective-permute-start = (bf16[2,128,128]{2,1,0:T(8,128)(2,1)S(1)}, bf16[2,128,128]{2,1,0:T(8,128)(2,1)S(1)}, u32[]{:S(2)}, u32[]{:S(2)}) collective-permute-start(bf16[2,128,128]{2,1,0:T(8,128)(2,1)S(1)} %get-tuple-element.158), channel_id=1, source_target_pairs={{0,4},{4,8},{8,12},{12,16},{16,20},{20,24},{24,28},{28,32},{32,36}... | collective-permute-start | bytes 196616 | tf_op jit(solution)/shard_map/ppermute | solution.py:25
  13.8 5.6 %collective-permute-start.1 = (bf16[2,128,128]{2,1,0:T(8,128)(2,1)S(1)}, bf16[2,128,128]{2,1,0:T(8,128)(2,1)S(1)}, u32[]{:S(2)}, u32[]{:S(2)}) collective-permute-start(bf16[2,128,128]{2,1,0:T(8,128)(2,1)S(1)} %get-tuple-element.159), channel_id=1, source_target_pairs={{4,0},{8,4},{12,8},{16,12},{20,16},{24,20},{28,24},{32,28},{36,32}... | collective-permute-start | bytes 196616 | tf_op jit(solution)/shard_map/ppermute | solution.py:27
  24.1 1.0 copy-start.7
  25.1 0.8 copy-start.8
  29.6 1.0 copy-start.7
  30.7 0.8 copy-start.8
  33.8 8.8 %copy-start.4 = (bf16[512,2048]{1,0:T(8,128)(2,1)}, bf16[512,2048]{1,0:T(8,128)(2,1)S(1)}, u32[]{:S(2)}) copy-start(bf16[512,2048]{1,0:T(8,128)(2,1)S(1)} %convolution_convert_fusion.1) | copy-start | bytes 6291460
  33.9 7.4 %collective-permute-start.2 = (bf16[64,2048]{1,0:T(8,128)(2,1)S(1)}, bf16[64,2048]{1,0:T(8,128)(2,1)S(1)}, u32[]{:S(2)}, u32[]{:S(2)}) collective-permute-start(bf16[64,2048]{1,0:T(8,128)(2,1)S(1)} %get-tuple-element.150), channel_id=1, source_target_pairs={{0,1},{1,2},{2,3},{3,0},{4,5},{5,6},{6,7},{7,4},{8,9},{9,10},{10,1... | collective-permute-start | bytes 786440 | tf_op jit(solution)/shard_map/ppermute | solution.py:67
  35.3 6.4 %collective-permute-start.4 = (bf16[64,2048]{1,0:T(8,128)(2,1)S(1)}, bf16[64,2048]{1,0:T(8,128)(2,1)S(1)}, u32[]{:S(2)}, u32[]{:S(2)}) collective-permute-start(bf16[64,2048]{1,0:T(8,128)(2,1)S(1)} %get-tuple-element.152), channel_id=1, source_target_pairs={{0,3},{1,0},{2,1},{3,2},{4,7},{5,4},{6,5},{7,6},{8,11},{9,8},{10,9... | collective-permute-start | bytes 786440 | tf_op jit(solution)/shard_map/ppermute | solution.py:67
  42.6 14.0 %collective-permute-start.5 = (bf16[128,2048]{1,0:T(8,128)(2,1)}, bf16[128,2048]{1,0:T(8,128)(2,1)S(1)}, u32[]{:S(2)}, u32[]{:S(2)}) collective-permute-start(bf16[128,2048]{1,0:T(8,128)(2,1)} %pad_maximum_fusion.3), channel_id=1, source_target_pairs={{0,3},{1,0},{2,1},{3,2},{4,7},{5,4},{6,5},{7,6},{8,11},{9,8},{10,9... | collective-permute-start | bytes 1572872 | tf_op jit(solution)/shard_map/ppermute | solution.py:67
  45.2 17.1 %copy-start.6 = (f32[2048]{0:T(1024)S(1)}, f32[2048]{0:T(1024)}, u32[]{:S(2)}) copy-start(f32[2048]{0:T(1024)} %param.17) | copy-start | bytes 24580
  46.1 14.7 %collective-permute-start.3 = (bf16[128,2048]{1,0:T(8,128)(2,1)}, bf16[128,2048]{1,0:T(8,128)(2,1)S(1)}, u32[]{:S(2)}, u32[]{:S(2)}) collective-permute-start(bf16[128,2048]{1,0:T(8,128)(2,1)} %pad_maximum_fusion.2), channel_id=1, source_target_pairs={{0,1},{1,2},{2,3},{3,0},{4,5},{5,6},{6,7},{7,4},{8,9},{9,10},{10,1... | collective-permute-start | bytes 1572872 | tf_op jit(solution)/shard_map/ppermute | solution.py:67
  62.3 23.1 %copy-start.2 = (f32[128,2048]{1,0:T(8,128)}, f32[128,2048]{1,0:T(8,128)S(1)}, u32[]{:S(2)}) copy-start(f32[128,2048]{1,0:T(8,128)S(1)} %get-tuple-element.141) | copy-start | bytes 3145732
  62.5 14.6 %collective-permute-start.7 = (bf16[128,2048]{1,0:T(8,128)(2,1)S(1)}, bf16[128,2048]{1,0:T(8,128)(2,1)S(1)}, u32[]{:S(2)}, u32[]{:S(2)}) collective-permute-start(bf16[128,2048]{1,0:T(8,128)(2,1)S(1)} %multiply_convert_fusion), channel_id=1, source_target_pairs={{0,1},{1,2},{2,3},{3,0},{4,5},{5,6},{6,7},{7,4},{8,9},{9,10},{10,1... | collective-permute-start | bytes 1572872 | tf_op jit(solution)/shard_map/ppermute | solution.py:67
  62.6 14.6 %collective-permute-start.6 = (bf16[128,2048]{1,0:T(8,128)(2,1)S(1)}, bf16[128,2048]{1,0:T(8,128)(2,1)S(1)}, u32[]{:S(2)}, u32[]{:S(2)}) collective-permute-start(bf16[128,2048]{1,0:T(8,128)(2,1)S(1)} %multiply_convert_fusion), channel_id=1, source_target_pairs={{0,3},{1,0},{2,1},{3,2},{4,7},{5,4},{6,5},{7,6},{8,11},{9,8},{10,9... | collective-permute-start | bytes 1572872 | tf_op jit(solution)/shard_map/ppermute | solution.py:67
  77.2 8.2 %collective-permute-start.8 = (bf16[64,2048]{1,0:T(8,128)(2,1)S(1)}, bf16[64,2048]{1,0:T(8,128)(2,1)S(1)}, u32[]{:S(2)}, u32[]{:S(2)}) collective-permute-start(bf16[64,2048]{1,0:T(8,128)(2,1)S(1)} %get-tuple-element.156), channel_id=1, source_target_pairs={{0,1},{1,2},{2,3},{3,0},{4,5},{5,6},{6,7},{7,4},{8,9},{9,10},{10,1... | collective-permute-start | bytes 786440 | tf_op jit(solution)/shard_map/ppermute | solution.py:67
  77.3 8.1 %collective-permute-start.9 = (bf16[64,2048]{1,0:T(8,128)(2,1)S(1)}, bf16[64,2048]{1,0:T(8,128)(2,1)S(1)}, u32[]{:S(2)}, u32[]{:S(2)}) collective-permute-start(bf16[64,2048]{1,0:T(8,128)(2,1)S(1)} %get-tuple-element.154), channel_id=1, source_target_pairs={{0,3},{1,0},{2,1},{3,2},{4,7},{5,4},{6,5},{7,6},{8,11},{9,8},{10,9... | collective-permute-start | bytes 786440 | tf_op jit(solution)/shard_map/ppermute | solution.py:67
  114.8 1.2 copy-start.1
  124.6 10.8 %collective-permute-start.12 = (bf16[64,2048]{1,0:T(8,128)(2,1)S(1)}, bf16[64,2048]{1,0:T(8,128)(2,1)S(1)}, u32[]{:S(2)}, u32[]{:S(2)}) collective-permute-start(bf16[64,2048]{1,0:T(8,128)(2,1)S(1)} %get-tuple-element.113), channel_id=1, source_target_pairs={{0,1},{1,2},{2,3},{3,0},{4,5},{5,6},{6,7},{7,4},{8,9},{9,10},{10,1... | collective-permute-start | bytes 786440 | tf_op jit(solution)/shard_map/ppermute | solution.py:67
  126.0 15.6 %collective-permute-start.10 = (bf16[64,2048]{1,0:T(8,128)(2,1)S(1)}, bf16[64,2048]{1,0:T(8,128)(2,1)S(1)}, u32[]{:S(2)}, u32[]{:S(2)}) collective-permute-start(bf16[64,2048]{1,0:T(8,128)(2,1)S(1)} %get-tuple-element.110), channel_id=1, source_target_pairs={{0,3},{1,0},{2,1},{3,2},{4,7},{5,4},{6,5},{7,6},{8,11},{9,8},{10,9... | collective-permute-start | bytes 786440 | tf_op jit(solution)/shard_map/ppermute | solution.py:67
  127.3 14.3 %collective-permute-start.11 = (bf16[64,2048]{1,0:T(8,128)(2,1)S(1)}, bf16[64,2048]{1,0:T(8,128)(2,1)S(1)}, u32[]{:S(2)}, u32[]{:S(2)}) collective-permute-start(bf16[64,2048]{1,0:T(8,128)(2,1)S(1)} %get-tuple-element.111), channel_id=1, source_target_pairs={{0,1},{1,2},{2,3},{3,0},{4,5},{5,6},{6,7},{7,4},{8,9},{9,10},{10,1... | collective-permute-start | bytes 786440 | tf_op jit(solution)/shard_map/ppermute | solution.py:67
  127.4 11.5 %collective-permute-start.14 = (bf16[64,2048]{1,0:T(8,128)(2,1)S(1)}, bf16[64,2048]{1,0:T(8,128)(2,1)S(1)}, u32[]{:S(2)}, u32[]{:S(2)}) collective-permute-start(bf16[64,2048]{1,0:T(8,128)(2,1)S(1)} %get-tuple-element.115), channel_id=1, source_target_pairs={{0,3},{1,0},{2,1},{3,2},{4,7},{5,4},{6,5},{7,6},{8,11},{9,8},{10,9... | collective-permute-start | bytes 786440 | tf_op jit(solution)/shard_map/ppermute | solution.py:67
  135.4 6.3 %copy-start.3 = (f32[128,2048]{1,0:T(8,128)S(1)}, f32[128,2048]{1,0:T(8,128)}, u32[]{:S(2)}) copy-start(f32[128,2048]{1,0:T(8,128)} %copy-done.2) | copy-start | bytes 3145732
  135.4 8.5 %collective-permute-start.13 = (bf16[64,2048]{1,0:T(8,128)(2,1)S(1)}, bf16[64,2048]{1,0:T(8,128)(2,1)S(1)}, u32[]{:S(2)}, u32[]{:S(2)}) collective-permute-start(bf16[64,2048]{1,0:T(8,128)(2,1)S(1)} %add_convert_fusion.2), channel_id=1, source_target_pairs={{0,1},{1,2},{2,3},{3,0},{4,5},{5,6},{6,7},{7,4},{8,9},{9,10},{10,1... | collective-permute-start | bytes 786440 | tf_op jit(solution)/shard_map/ppermute | solution.py:67
  139.0 6.9 %collective-permute-start.15 = (bf16[64,2048]{1,0:T(8,128)(2,1)S(1)}, bf16[64,2048]{1,0:T(8,128)(2,1)S(1)}, u32[]{:S(2)}, u32[]{:S(2)}) collective-permute-start(bf16[64,2048]{1,0:T(8,128)(2,1)S(1)} %add_convert_fusion.1), channel_id=1, source_target_pairs={{0,3},{1,0},{2,1},{3,2},{4,7},{5,4},{6,5},{7,6},{8,11},{9,8},{10,9... | collective-permute-start | bytes 786440 | tf_op jit(solution)/shard_map/ppermute | solution.py:67
Sparse Core Ops, SparseCore 0:
  10.1 104.6 all-gather.1
